TPU v7x, 512 devices: a whole 4x4x16 slice. The times are simulated.
512 devices in a mesh: kv: 64 (over z, y), tp: 8 (over x, core).
Axes of the slice: x: 4, y: 4, z: 16, core: 2. Of those that a mesh axis runs over, the one named last changes fastest.
Arguments:
- queries: bfloat16 [16384, 1024], P('kv', 'tp'), may hold values from -4 to 4
- keys: bfloat16 [16384, 1024], P('kv', 'tp'), may hold values from -4 to 4
- values: bfloat16 [16384, 1024], P('kv', 'tp'), may hold values from -5 to 5
- log_sums: float32 [16, 16384], P('tp', 'kv'), may hold values from 5.5 to 7
- out_grad: bfloat16 [16384, 1024], P('kv', 'tp'), may hold values from -24 to 24
- chosen: int32 [128, 8], P('kv'), may hold values from -1 to 511, as said below
- normed: bfloat16 [16384, 2048], P('kv', 'tp'), may hold values from -0.23925781 to 0.23925781
Outputs:
- query_grad: bfloat16 [16384, 1024], P('kv', 'tp')
- key_grad: bfloat16 [16384, 1024], P('kv', 'tp')
- value_grad: bfloat16 [16384, 1024], P('kv', 'tp')
- weight_grad: float32 [2048, 1024], P('kv', 'tp')
Inputs may be any that keep to these rules, and one draw needn't show every extreme that they name: `chosen`: each used entry names a key block that ends at or before its query block's start; the used entries of one list are distinct. Among the lists of the 2 query blocks of one index of kv, the key blocks of any other index of kv appear as at most one distinct block; for every index from 1 on, the first query block's list names a block of the index before, and the last index's first query block's list names a block of index 0. Blocks of the own index of kv before the query block may appear freely.
All inputs are finite; a program needn't handle non-finite values.
Results may differ from a plain program's by a relative error of at most 0.008.
Values may be sent and summed in bfloat16 or wider, within the bound.
No kernel may reach another device: no remote copies, remote signals or barrier semaphores. Data moves between devices by JAX's collectives and lax.ppermute only.
A program may use at most 64 MiB of HBM per device.

v0:
```python
import jax
import jax.numpy as jnp
from jax import lax
from jax.experimental import pallas as pl
from jax.experimental.pallas import tpu as pltpu
from jax.sharding import Mesh
from jax.sharding import PartitionSpec as P


KV = ("z", "y")
QB = 128
KB = 32
HD = 64
SEL = 8
F32 = jnp.float32
BF16 = jnp.bfloat16


def iota(shape, dim):
    return lax.broadcasted_iota(jnp.int32, shape, dim)


def dot(a, b, dims=((1,), (0,))):
    return lax.dot_general(a, b, (dims, ((), ())), preferred_element_type=F32)


def one_hot(hits):
    return jnp.where(hits, 1.0, 0.0).astype(BF16)


def pack_kernel(base_ref, chosen_ref, keys_ref, values_ref, normed_ref, out_ref):
    lane = iota((1, 128), 1)
    high = jnp.zeros((1, 128), F32)
    low = jnp.zeros((1, 128), F32)
    for g in range(2):
        for s in range(SEL):
            entry = chosen_ref[g, s] + 1
            here = lane == base_ref[0] + (g * SEL + s)
            high = jnp.where(here, (entry >> 3).astype(F32), high)
            low = jnp.where(here, (entry & 7).astype(F32), low)
    row, col = iota((64 * 18, 512), 0), iota((64 * 18, 512), 1)
    piece = (row * 3641) >> 16
    kind = row - piece * 18
    source = jnp.where(kind < 8, kind * KB, 256 + (kind - 10) * KB) + (piece >> 1)
    perm = one_hot(((kind < 8) | (kind >= 10)) & (col == source))
    pairs = jnp.concatenate([keys_ref[...], values_ref[...]], axis=1)
    both = dot(perm, jnp.concatenate([pairs, normed_ref[...]], axis=0))
    row = iota((64 * 18, 128), 0)
    piece = (row * 3641) >> 16
    kind = row - piece * 18
    extra = jnp.where(kind == 8, high, 0.0) + jnp.where(kind == 9, low, 0.0)
    out_ref[...] = (jnp.where((piece & 1) == 0, both[:, :128], both[:, 128:]) + extra).astype(BF16)


def select_kernel(got_ref, out_ref, ids_ref):
    got = got_ref[...]
    group, col = iota((8, 64 * 18), 0) * 144, iota((8, 64 * 18), 1)
    kind = col - ((col * 3641) >> 16) * 18
    inside = (col >= group) & (col < group + 144)
    ids = dot(one_hot(inside & (kind == 8)), got) * 8.0 + dot(one_hot(inside & (kind == 9)), got)
    ids_ref[...] = ids
    entry = ids.astype(jnp.int32) - 1
    columns = jnp.where(entry >= 0, entry + (entry >> 3) * 10, -1).astype(F32).T
    number = iota((128, 64 * 18), 1).astype(F32)
    for j in range(8):
        hot = one_hot(number == columns[:, j : j + 1])
        out_ref[j * 128 : (j + 1) * 128, :] = dot(hot, got).astype(BF16)


def half_kernel(got_ref, out_ref):
    row, col = iota((512, 64 * 18), 0), iota((512, 64 * 18), 1)
    out_ref[...] = dot(one_hot(col == row + (row >> 3) * 10 + 10), got_ref[...]).astype(BF16)


def turn_kernel(place_ref, mine_ref, other_ref, normed_ref, out_ref):
    eye = one_hot(iota((512, 512), 0) == iota((512, 512), 1))
    half = place_ref[0] & 1
    out_ref[half, :, 256:] = dot(mine_ref[...], eye, ((0,), (0,))).astype(BF16)
    out_ref[1 - half, :, 256:] = dot(other_ref[...], eye, ((0,), (0,))).astype(BF16)
    out_ref[:, :, :256] = dot(normed_ref[...], eye[:256, :256], ((0,), (0,))).astype(BF16).reshape(2, 128, 256)


def attend_kernel(
    chosen_ref, queries_ref, keys_ref, values_ref, grad_ref, sums_ref, got_ref, dq_ref, back_ref, own_ref
):
    mine = (iota((2 * QB, 128), 1) >= HD) == (iota((2 * QB, 128), 0) >= QB)
    causal = iota((QB, 2 * QB), 0) <= (iota((QB, 2 * QB), 1) & (QB - 1))
    sub = iota((SEL, 2 * QB), 0)
    low_lanes = iota((QB, 128), 1) < HD
    for g in range(2):
        span = slice(g * QB, (g + 1) * QB)
        picked = []
        for n in range(2):
            got = got_ref[:, n].astype(F32)[:, g * SEL : (g + 1) * SEL, :]
            picked.append(got.reshape(KB * SEL, 128).astype(BF16))
        keys = jnp.concatenate([picked[0], keys_ref[span, :]], axis=0)
        values = jnp.concatenate([picked[1], values_ref[span, :]], axis=0)
        q = queries_ref[span, :].astype(F32) * (HD**-0.5)
        do = grad_ref[span, :].astype(F32)
        q = jnp.where(mine, jnp.concatenate([q, q], axis=0), 0.0).astype(BF16)
        do = jnp.where(mine, jnp.concatenate([do, do], axis=0), 0.0).astype(BF16)
        sums = jnp.concatenate([sums_ref[0:1, span], sums_ref[1:2, span]], axis=1)
        used = jnp.zeros((SEL, 2 * QB), jnp.int32)
        for s in range(SEL):
            used = jnp.where(sub == s, chosen_ref[g, s] + 1, used)
        used = (used > 0)[None]
        scores = dot(keys, q, ((1,), (1,)))
        dots = dot(values, do, ((1,), (1,)))
        raw = jnp.exp(scores - sums)
        picked = jnp.where(used, raw[: KB * SEL].reshape(KB, SEL, 2 * QB), 0.0).reshape(KB * SEL, 2 * QB)
        weights = jnp.concatenate([picked, jnp.where(causal, raw[KB * SEL :], 0.0)], axis=0)
        low = weights.astype(BF16)
        deltas = jnp.sum(low.astype(F32) * dots, axis=0, keepdims=True)
        slopes = (weights * (dots - deltas)).astype(BF16)
        dk = dot(slopes, q)
        dv = dot(low, do)
        dq = dot(slopes, keys, ((0,), (0,)))
        back_ref[:, 0, g * SEL : (g + 1) * SEL, :] = dk[: KB * SEL].reshape(KB, SEL, 128).astype(BF16)
        back_ref[:, 1, g * SEL : (g + 1) * SEL, :] = dv[: KB * SEL].reshape(KB, SEL, 128).astype(BF16)
        own_ref[0, span, :] = dk[KB * SEL :].astype(BF16)
        own_ref[1, span, :] = dv[KB * SEL :].astype(BF16)
        dq_ref[span, :] = (jnp.where(low_lanes, dq[:QB], dq[QB:]) * (HD**-0.5)).astype(BF16)


def sum_kernel(place_ref, ids_ref, got_ref, own_ref, mine_ref, other_ref, out_ref):
    number = (iota((512, 128), 0) + 1).astype(F32)
    sums = jnp.zeros((512, 128), F32)
    for j in range(8):
        hot = one_hot(number == ids_ref[j : j + 1, :])
        sums = sums + dot(hot, got_ref[j * 128 : (j + 1) * 128, :])
    held = jnp.where((place_ref[0] & 1) == 1, sums, 0.0).astype(BF16)
    value = jnp.concatenate([own_ref[1], held], axis=0)
    for c, features_ref in enumerate((mine_ref, other_ref)):
        for s in range(4):
            t = ((place_ref[1] - s) & 3) * 2 + ((place_ref[2] + c) & 1)
            part = dot(features_ref[s].reshape(256, 768), value).astype(BF16).reshape(2, 4, 32, 128)
            for zz in range(2):
                for y in range(4):
                    out_ref[y, t * 2 + zz] = part[zz, y]
    sums = sums.reshape(4, 4, 4, 8, 128)
    for y in range(4):
        out_ref[y, 16:] = sums[:, :, y].reshape(4, 32, 128).astype(BF16)


def middle_kernel(got_ref, out_ref):
    total = got_ref[0, :16].astype(F32)
    for y in range(1, 4):
        total = total + got_ref[y, :16].astype(F32)
    out_ref[:, :32] = total.astype(BF16)
    sums = [got_ref[y, 16:].astype(F32).reshape(16, 8, 128) for y in range(4)]
    out_ref[:, 32:] = jnp.concatenate(sums, axis=1).astype(BF16)


def last_kernel(got_ref, own_ref, dk_ref, dv_ref, total_ref):
    total_ref[...] = got_ref[:, :32].astype(F32).sum(axis=0)
    sums = got_ref[:, 32:].reshape(512, 128)
    row, col = iota((256, 512), 0), iota((256, 512), 1)
    first = (row & 31) * 16 + (row >> 5)
    dk_ref[...] = (dot(one_hot(col == first), sums) + own_ref[0].astype(F32)).astype(BF16)
    dv_ref[...] = (dot(one_hot(col == first + 8), sums) + own_ref[1].astype(F32)).astype(BF16)


VM = pl.BlockSpec(memory_space=pltpu.VMEM)
SM = pl.BlockSpec(memory_space=pltpu.SMEM)


def call(kernel, out, specs, *args, inputs=True, hbm=(), limit=0):
    if inputs:
        args = [pltpu.with_memory_space_constraint(a, pltpu.VMEM) if s is VM else a for a, s in zip(args, specs)]
    return pl.pallas_call(
        kernel,
        out_shape=[o if n in hbm else pltpu.VMEM(o.shape, o.dtype) for n, o in enumerate(out)],
        in_specs=specs,
        out_specs=[VM] * len(out),
        compiler_params=pltpu.CompilerParams(vmem_limit_bytes=limit << 20 if limit else None),
    )(*args)


def shape(*dims, dtype=BF16):
    return jax.ShapeDtypeStruct(dims, dtype)


def exchange(x, axis):
    return lax.all_to_all(x, axis, split_axis=0, concat_axis=0, tiled=True)


def shift(x, axis, by):
    size = lax.axis_size(axis)
    return lax.ppermute(x, axis, [(n, (n + by) % size) for n in range(size)])


def body(queries, keys, values, log_sums, out_grad, chosen, normed):
    rows = queries.shape[0]
    base = ((lax.axis_index("z") * 4 + lax.axis_index("y")) & 7) * 16
    base = base.astype(jnp.int32).reshape(1)
    place = jnp.stack([lax.axis_index("y"), lax.axis_index("x"), lax.axis_index("c")]).astype(jnp.int32)
    (pieces,) = call(
        pack_kernel, [shape(1152, 128)], [SM, SM] + [VM] * 3, base, chosen, keys, values, normed, inputs=False
    )
    pieces = exchange(pieces.reshape(64, 9, 2, 128), KV).reshape(1152, 128)
    picked, ids = call(select_kernel, [shape(1024, 128), shape(8, 128, dtype=F32)], [VM], pieces)
    picked = exchange(picked.reshape(64, 16, 128), KV)
    (half,) = call(half_kernel, [shape(512, 128)], [VM], pieces)
    other = lax.ppermute(half, "y", [(n, n ^ 1) for n in range(4)])
    (features,) = call(turn_kernel, [shape(2, 128, 768)], [SM] + [VM] * 3, place, half, other, normed)
    parts = [features]
    for s in range(1, 4):
        parts.append(shift(features, "x", s))
    features = jnp.stack(parts)
    others = shift(features, "c", 1)
    query_grad, back, own = call(
        attend_kernel,
        [shape(rows, 128), shape(KB, 2, 16, 128), shape(2, rows, 128)],
        [SM] + [VM] * 6,
        chosen, queries, keys, values, out_grad, log_sums, picked.reshape(KB, 2, 16, 128),
        hbm=(0,),
    )
    back = exchange(back.reshape(64, 16, 128), KV)
    (sums,) = call(
        sum_kernel,
        [shape(4, 20, 32, 128)],
        [SM] + [VM] * 5,
        place, ids, back.reshape(1024, 128), own, features, others,
        limit=24,
    )
    sums = exchange(sums, "y")
    (sums,) = call(middle_kernel, [shape(16, 64, 128)], [VM], sums)
    sums = exchange(sums, "z")
    key_grad, value_grad, weight_grad = call(
        last_kernel,
        [shape(rows, 128), shape(rows, 128), shape(32, 128, dtype=F32)],
        [VM] * 2,
        sums, own,
        hbm=(0, 1, 2),
    )
    return query_grad, key_grad, value_grad, weight_grad


def solution(mesh):
    fine = Mesh(mesh.devices.reshape(16, 4, 4, 2), ("z", "y", "x", "c"))
    both = P(KV, ("x", "c"))
    in_specs = (both, both, both, P(("x", "c"), KV), both, P(KV, None), both)
    return jax.shard_map(body, mesh=fine, in_specs=in_specs, out_specs=(both,) * 4, check_vma=False)
```

profile of v0, /device:TPU:36, one launch (start us, length us, event | category | flops | bytes accessed | tf_op | source)
XLA Modules:
  0.0 153.5 jit_solution(4619386313961939936)
XLA Ops:
  0.6 0.0 copy-start
  0.6 1.8 %shard_map.102 = bf16[1152,128]{1,0:T(8,128)(2,1)S(1)} custom-call(s32[1]{0:T(128)} %bitcast.base_ref, s32[2,8]{1,0:T(2,128)} %chosen_ref.3, bf16[256,128]{1,0:T(8,128)(2,1)} %keys_ref.3, bf16[256,128]{1,0:T(8,128)(2,1)} %values_ref.3, bf16[256,256]{1,0:T(8,128)(2,1)} %normed_ref.3), custom_call_target="tpu_custom_call" | custom-call | tf_op jit(solution)/shard_map/pallas_call | solution.py:170
  2.5 41.3 %all_to_all.25 = bf16[64,9,2,128]{3,2,1,0:T(2,128)(2,1)S(1)} all-to-all(bf16[64,9,2,128]{3,2,1,0:T(2,128)(2,1)S(1)} %bitcast.17), channel_id=1, replica_groups=mesh['z'=16,'y'=4,'x'=4,'c'=2] {'z','y'}, dimensions={0} | all-to-all | bytes 589824 | tf_op jit(solution)/shard_map/all_to_all | solution.py:184
  43.8 0.5 shard_map.105.mine_ref
  44.3 2.7 %collective-permute-start = (bf16[512,128]{1,0:T(8,128)(2,1)S(1)}, bf16[512,128]{1,0:T(8,128)(2,1)S(1)}, u32[]{:S(2)}, u32[]{:S(2)}) collective-permute-start(bf16[512,128]{1,0:T(8,128)(2,1)S(1)} %shard_map.105.mine_ref), channel_id=1, source_target_pairs={{0,8},{8,0},{16,24},{24,16},{1,9},{9,1},{17,25},{25,17},{2,10},{10... | collective-permute-start | bytes 393224 | tf_op jit(solution)/shard_map/ppermute | solution.py:204
  47.0 0.6 pad_add_fusion.place_ref
  47.6 3.5 %collective-permute-done.other_ref = bf16[512,128]{1,0:T(8,128)(2,1)S(1)} collective-permute-done((bf16[512,128]{1,0:T(8,128)(2,1)S(1)}, bf16[512,128]{1,0:T(8,128)(2,1)S(1)}, u32[]{:S(2)}, u32[]{:S(2)}) %collective-permute-start) | collective-permute-done | bytes 131104 | tf_op jit(solution)/shard_map/ppermute | solution.py:204
  51.2 0.0 copy-done
  51.2 1.0 shard_map.106
  52.2 2.4 %collective-permute-start.3 = (bf16[2,128,768]{2,1,0:T(8,128)(2,1)S(1)}, bf16[2,128,768]{2,1,0:T(8,128)(2,1)S(1)}, u32[]{:S(2)}, u32[]{:S(2)}) collective-permute-start(bf16[2,128,768]{2,1,0:T(8,128)(2,1)S(1)} %shard_map.106), channel_id=1, source_target_pairs={{0,6},{2,0},{4,2},{6,4},{1,7},{3,1},{5,3},{7,5},{8,14},{10,8},{12,... | collective-permute-start | bytes 1179656 | tf_op jit(solution)/shard_map/ppermute | solution.py:189
  54.7 4.6 %collective-permute-start.2 = (bf16[2,128,768]{2,1,0:T(8,128)(2,1)S(1)}, bf16[2,128,768]{2,1,0:T(8,128)(2,1)S(1)}, u32[]{:S(2)}, u32[]{:S(2)}) collective-permute-start(bf16[2,128,768]{2,1,0:T(8,128)(2,1)S(1)} %shard_map.106), channel_id=1, source_target_pairs={{0,4},{2,6},{4,0},{6,2},{1,5},{3,7},{5,1},{7,3},{8,12},{10,14},{12... | collective-permute-start | bytes 1179656 | tf_op jit(solution)/shard_map/ppermute | solution.py:189
  59.3 1.9 %collective-permute-start.1 = (bf16[2,128,768]{2,1,0:T(8,128)(2,1)S(1)}, bf16[2,128,768]{2,1,0:T(8,128)(2,1)S(1)}, u32[]{:S(2)}, u32[]{:S(2)}) collective-permute-start(bf16[2,128,768]{2,1,0:T(8,128)(2,1)S(1)} %shard_map.106), channel_id=1, source_target_pairs={{0,2},{2,4},{4,6},{6,0},{1,3},{3,5},{5,7},{7,1},{8,10},{10,12},{12... | collective-permute-start | bytes 1179656 | tf_op jit(solution)/shard_map/ppermute | solution.py:189
  61.2 1.8 %shard_map.103 = (bf16[1024,128]{1,0:T(8,128)(2,1)}, f32[8,128]{1,0:T(8,128)S(1)}) custom-call(bf16[1152,128]{1,0:T(8,128)(2,1)S(1)} %bitcast.15), custom_call_target="tpu_custom_call" | custom-call | tf_op jit(solution)/shard_map/pallas_call | solution.py:170
  63.1 5.7 %all-to-all-start.1 = ((bf16[64,16,128]{2,1,0:T(8,128)(2,1)}), bf16[64,16,128]{2,1,0:T(8,128)(2,1)S(1)}, u32[]{:S(2)}, u32[]{:S(2)}) async-start(bf16[64,16,128]{2,1,0:T(8,128)(2,1)} %bitcast.3), calls=%async_computation.1 | async-start | bytes 524288 | tf_op jit(solution)/shard_map/all_to_all | solution.py:184
  68.7 0.0 collective-permute-done.3
  68.7 0.0 collective-permute-done.2
  68.8 4.1 %collective-permute-done.1 = bf16[2,128,768]{2,1,0:T(8,128)(2,1)S(1)} collective-permute-done((bf16[2,128,768]{2,1,0:T(8,128)(2,1)S(1)}, bf16[2,128,768]{2,1,0:T(8,128)(2,1)S(1)}, u32[]{:S(2)}, u32[]{:S(2)}) %collective-permute-start.1) | collective-permute-done | bytes 393248 | tf_op jit(solution)/shard_map/ppermute | solution.py:189
  72.8 0.0 copy-start.7
  72.8 0.8 copy-done.7
  73.6 0.0 copy-start.1
  73.6 0.0 copy-start.2
  73.6 0.0 copy-start.3
  73.6 0.0 copy-start.4
  73.6 0.0 copy-start.6
  73.6 0.0 copy-start.5
  73.6 1.2 pad_maximum_fusion.mine_ref
  74.9 1.9 %collective-permute-start.4 = (bf16[4,2,128,768]{3,2,1,0:T(8,128)(2,1)S(1)}, bf16[4,2,128,768]{3,2,1,0:T(8,128)(2,1)}, u32[]{:S(2)}, u32[]{:S(2)}) collective-permute-start(bf16[4,2,128,768]{3,2,1,0:T(8,128)(2,1)S(1)} %pad_maximum_fusion.mine_ref), channel_id=1, source_target_pairs={{0,1},{1,0},{2,3},{3,2},{4,5},{5,4},{6,7},{7,6},{8,9},{9,8},{10,11... | collective-permute-start | bytes 4718600 | tf_op jit(solution)/shard_map/ppermute | solution.py:189
  76.8 11.4 %all-to-all-done.1 = bf16[64,16,128]{2,1,0:T(8,128)(2,1)S(1)} async-done(((bf16[64,16,128]{2,1,0:T(8,128)(2,1)}), bf16[64,16,128]{2,1,0:T(8,128)(2,1)S(1)}, u32[]{:S(2)}, u32[]{:S(2)}) %all-to-all-start.1) | async-done | bytes 262176 | tf_op jit(solution)/shard_map/all_to_all | solution.py:184
  88.1 0.0 copy-done.1
  88.1 0.0 copy-done.2
  88.1 0.0 copy-done.3
  88.2 0.0 copy-done.4
  88.2 0.0 copy-done.6
  88.2 2.4 %shard_map.104 = (bf16[256,128]{1,0:T(8,128)(2,1)}, bf16[32,2,16,128]{3,2,1,0:T(8,128)(2,1)S(1)}, bf16[2,256,128]{2,1,0:T(8,128)(2,1)S(1)}) custom-call(s32[2,8]{1,0:T(2,128)} %chosen_ref.3, bf16[256,128]{1,0:T(8,128)(2,1)S(1)} %copy-done.3, bf16[256,128]{1,0:T(8,128)(2,1)S(1)} %copy-done.1, bf16[256,128]{1,0:T(8,128)(2,1)S(1)} %copy-done.2, ...), custom_call_target="tpu_custom_call" | custom-call | tf_op jit(solution)/shard_map/pallas_call | solution.py:170
  90.6 25.0 %all_to_all.26 = bf16[64,16,128]{2,1,0:T(8,128)(2,1)S(1)} all-to-all(bf16[64,16,128]{2,1,0:T(8,128)(2,1)S(1)} %bitcast.20), channel_id=1, replica_groups=mesh['z'=16,'y'=4,'x'=4,'c'=2] {'z','y'}, dimensions={0} | all-to-all | bytes 524288 | tf_op jit(solution)/shard_map/all_to_all | solution.py:184
  115.6 0.0 collective-permute-done.4.other_ref
  115.6 0.0 copy-done.5
  115.6 3.2 %shard_map.107 = bf16[4,20,32,128]{3,2,1,0:T(8,128)(2,1)S(1)} custom-call(s32[3]{0:T(128)S(1)} %copy-done.5, f32[8,128]{1,0:T(8,128)S(1)} %get-tuple-element.14.ids_ref, bf16[1024,128]{1,0:T(8,128)(2,1)S(1)} %bitcast.18, bf16[2,256,128]{2,1,0:T(8,128)(2,1)S(1)} %get-tuple-element.16.own_ref, bf16[4,2,128,768]{3,2,1,0:T(8,128)(2,1)S(1)} %pad_maximum_fusion.mine_ref, ...), custom_call_target="tpu_custom_call" | custom-call | tf_op jit(solution)/shard_map/pallas_call | solution.py:170
  118.8 12.0 %all_to_all.27.got_ref = bf16[4,20,32,128]{3,2,1,0:T(8,128)(2,1)S(1)} all-to-all(bf16[4,20,32,128]{3,2,1,0:T(8,128)(2,1)S(1)} %shard_map.107), channel_id=1, replica_groups=mesh['z'=16,'y'=4,'x'=4,'c'=2] {'y'}, dimensions={0} | all-to-all | bytes 1310720 | tf_op jit(solution)/shard_map/all_to_all | solution.py:184
  130.8 0.1 shard_map.108
  130.9 21.6 %all_to_all.28.got_ref = bf16[16,64,128]{2,1,0:T(8,128)(2,1)S(1)} all-to-all(bf16[16,64,128]{2,1,0:T(8,128)(2,1)S(1)} %shard_map.108), channel_id=1, replica_groups=mesh['z'=16,'y'=4,'x'=4,'c'=2] {'z'}, dimensions={0} | all-to-all | bytes 524288 | tf_op jit(solution)/shard_map/all_to_all | solution.py:184
  152.5 1.0 shard_map.109
Async XLA Ops:
  0.6 50.5 %copy-start = (bf16[256,256]{1,0:T(8,128)(2,1)S(1)}, bf16[256,256]{1,0:T(8,128)(2,1)}, u32[]{:S(2)}) copy-start(bf16[256,256]{1,0:T(8,128)(2,1)} %normed_ref.3) | copy-start | bytes 393220
  44.3 6.9 %collective-permute-start = (bf16[512,128]{1,0:T(8,128)(2,1)S(1)}, bf16[512,128]{1,0:T(8,128)(2,1)S(1)}, u32[]{:S(2)}, u32[]{:S(2)}) collective-permute-start(bf16[512,128]{1,0:T(8,128)(2,1)S(1)} %shard_map.105.mine_ref), channel_id=1, source_target_pairs={{0,8},{8,0},{16,24},{24,16},{1,9},{9,1},{17,25},{25,17},{2,10},{10... | collective-permute-start | bytes 393224 | tf_op jit(solution)/shard_map/ppermute | solution.py:204
  52.2 16.5 %collective-permute-start.3 = (bf16[2,128,768]{2,1,0:T(8,128)(2,1)S(1)}, bf16[2,128,768]{2,1,0:T(8,128)(2,1)S(1)}, u32[]{:S(2)}, u32[]{:S(2)}) collective-permute-start(bf16[2,128,768]{2,1,0:T(8,128)(2,1)S(1)} %shard_map.106), channel_id=1, source_target_pairs={{0,6},{2,0},{4,2},{6,4},{1,7},{3,1},{5,3},{7,5},{8,14},{10,8},{12,... | collective-permute-start | bytes 1179656 | tf_op jit(solution)/shard_map/ppermute | solution.py:189
  54.7 14.1 %collective-permute-start.2 = (bf16[2,128,768]{2,1,0:T(8,128)(2,1)S(1)}, bf16[2,128,768]{2,1,0:T(8,128)(2,1)S(1)}, u32[]{:S(2)}, u32[]{:S(2)}) collective-permute-start(bf16[2,128,768]{2,1,0:T(8,128)(2,1)S(1)} %shard_map.106), channel_id=1, source_target_pairs={{0,4},{2,6},{4,0},{6,2},{1,5},{3,7},{5,1},{7,3},{8,12},{10,14},{12... | collective-permute-start | bytes 1179656 | tf_op jit(solution)/shard_map/ppermute | solution.py:189
  59.3 13.5 %collective-permute-start.1 = (bf16[2,128,768]{2,1,0:T(8,128)(2,1)S(1)}, bf16[2,128,768]{2,1,0:T(8,128)(2,1)S(1)}, u32[]{:S(2)}, u32[]{:S(2)}) collective-permute-start(bf16[2,128,768]{2,1,0:T(8,128)(2,1)S(1)} %shard_map.106), channel_id=1, source_target_pairs={{0,2},{2,4},{4,6},{6,0},{1,3},{3,5},{5,7},{7,1},{8,10},{10,12},{12... | collective-permute-start | bytes 1179656 | tf_op jit(solution)/shard_map/ppermute | solution.py:189
  63.1 25.1 %all-to-all-start.1 = ((bf16[64,16,128]{2,1,0:T(8,128)(2,1)}), bf16[64,16,128]{2,1,0:T(8,128)(2,1)S(1)}, u32[]{:S(2)}, u32[]{:S(2)}) async-start(bf16[64,16,128]{2,1,0:T(8,128)(2,1)} %bitcast.3), calls=%async_computation.1 | async-start | bytes 524288 | tf_op jit(solution)/shard_map/all_to_all | solution.py:184
  72.8 0.8 copy-start.7
  73.6 14.6 %copy-start.1 = (bf16[256,128]{1,0:T(8,128)(2,1)S(1)}, bf16[256,128]{1,0:T(8,128)(2,1)}, u32[]{:S(2)}) copy-start(bf16[256,128]{1,0:T(8,128)(2,1)} %keys_ref.3) | copy-start | bytes 196612
  73.6 14.6 %copy-start.2 = (bf16[256,128]{1,0:T(8,128)(2,1)S(1)}, bf16[256,128]{1,0:T(8,128)(2,1)}, u32[]{:S(2)}) copy-start(bf16[256,128]{1,0:T(8,128)(2,1)} %values_ref.3) | copy-start | bytes 196612
  73.6 14.6 %copy-start.3 = (bf16[256,128]{1,0:T(8,128)(2,1)S(1)}, bf16[256,128]{1,0:T(8,128)(2,1)}, u32[]{:S(2)}) copy-start(bf16[256,128]{1,0:T(8,128)(2,1)} %queries_ref.1) | copy-start | bytes 196612
  73.6 14.6 %copy-start.4 = (bf16[256,128]{1,0:T(8,128)(2,1)S(1)}, bf16[256,128]{1,0:T(8,128)(2,1)}, u32[]{:S(2)}) copy-start(bf16[256,128]{1,0:T(8,128)(2,1)} %grad_ref.1) | copy-start | bytes 196612
  73.6 14.6 %copy-start.6 = (f32[2,256]{1,0:T(2,128)S(1)}, f32[2,256]{1,0:T(2,128)}, u32[]{:S(2)}) copy-start(f32[2,256]{1,0:T(2,128)} %sums_ref.1) | copy-start | bytes 6148
  73.6 42.0 %copy-start.5 = (s32[3]{0:T(128)S(1)}, s32[3]{0:T(128)}, u32[]{:S(2)}) copy-start(s32[3]{0:T(128)} %pad_add_fusion.place_ref) | copy-start | bytes 40
  74.9 40.7 %collective-permute-start.4 = (bf16[4,2,128,768]{3,2,1,0:T(8,128)(2,1)S(1)}, bf16[4,2,128,768]{3,2,1,0:T(8,128)(2,1)}, u32[]{:S(2)}, u32[]{:S(2)}) collective-permute-start(bf16[4,2,128,768]{3,2,1,0:T(8,128)(2,1)S(1)} %pad_maximum_fusion.mine_ref), channel_id=1, source_target_pairs={{0,1},{1,0},{2,3},{3,2},{4,5},{5,4},{6,7},{7,6},{8,9},{9,8},{10,11... | collective-permute-start | bytes 4718600 | tf_op jit(solution)/shard_map/ppermute | solution.py:189
where the time goes:
time: 154 us; the launch traced here: 153 us
  blocking collectives  100 us (65%)
  starting transfers between devices  19.3 us (13%)
  waiting for transfers between devices  19 us (12%)
  Pallas kernels  11.8 us (8%)
  other arithmetic  1.84 us (1%)
    all_to_all x4, blocking collectives, exchange(): return lax.all_to_all(x, axis, split_axis=0, concat_axis=0, tiled=True)  100 us
    pallas_call x8, Pallas kernels, call(): pl.pallas_call(kernel, out_shape=[o if n in hbm else pltpu.VMEM(o.shape,...  11.8 us
    all_to_all x1, waiting for transfers between devices, exchange(): return lax.all_to_all(x, axis, split_axis=0, concat_axis=0, tiled=True)  11.4 us
    ppermute x4, starting transfers between devices, shift(): return lax.ppermute(x, axis, [(n, (n + by) % size) for n in range(size)])  10.9 us
    all_to_all x1, starting transfers between devices, exchange(): return lax.all_to_all(x, axis, split_axis=0, concat_axis=0, tiled=True)  5.67 us
    ppermute x4, waiting for transfers between devices, shift(): return lax.ppermute(x, axis, [(n, (n + by) % size) for n in range(size)])  4.07 us
    ppermute x1, waiting for transfers between devices, body(): other = lax.ppermute(half, 'y', [(n, n ^ 1) for n in range(4)])  3.53 us
  transfers between devices with their start and end apart: 6, of which 3 were waited for; matrix products, arithmetic and copies ran while one was open for 1% of the time, Pallas kernels for 3%

commit v1 on v0

--- a/solution.py
+++ b/solution.py
@@ -72,12 +72,17 @@
     out_ref[...] = dot(one_hot(col == row + (row >> 3) * 10 + 10), got_ref[...]).astype(BF16)
 
 
-def turn_kernel(place_ref, mine_ref, other_ref, normed_ref, out_ref):
+def turn_own_kernel(normed_ref, out_ref):
+    eye = one_hot(iota((256, 256), 0) == iota((256, 256), 1))
+    out_ref[...] = dot(normed_ref[...], eye, ((0,), (0,))).astype(BF16)
+
+
+def turn_kernel(y_ref, mine_ref, other_ref, own_ref, out_ref):
     eye = one_hot(iota((512, 512), 0) == iota((512, 512), 1))
-    half = place_ref[0] & 1
+    half = y_ref[0] & 1
     out_ref[half, :, 256:] = dot(mine_ref[...], eye, ((0,), (0,))).astype(BF16)
     out_ref[1 - half, :, 256:] = dot(other_ref[...], eye, ((0,), (0,))).astype(BF16)
-    out_ref[:, :, :256] = dot(normed_ref[...], eye[:256, :256], ((0,), (0,))).astype(BF16).reshape(2, 128, 256)
+    out_ref[:, :, :256] = own_ref[...].reshape(2, 128, 256)
 
 
 def attend_kernel(
@@ -122,17 +127,17 @@
         dq_ref[span, :] = (jnp.where(low_lanes, dq[:QB], dq[QB:]) * (HD**-0.5)).astype(BF16)
 
 
-def sum_kernel(place_ref, ids_ref, got_ref, own_ref, mine_ref, other_ref, out_ref):
+def sum_kernel(y_ref, x_ref, c_ref, ids_ref, got_ref, own_ref, mine_ref, other_ref, out_ref):
     number = (iota((512, 128), 0) + 1).astype(F32)
     sums = jnp.zeros((512, 128), F32)
     for j in range(8):
         hot = one_hot(number == ids_ref[j : j + 1, :])
         sums = sums + dot(hot, got_ref[j * 128 : (j + 1) * 128, :])
-    held = jnp.where((place_ref[0] & 1) == 1, sums, 0.0).astype(BF16)
+    held = jnp.where((y_ref[0] & 1) == 1, sums, 0.0).astype(BF16)
     value = jnp.concatenate([own_ref[1], held], axis=0)
     for c, features_ref in enumerate((mine_ref, other_ref)):
         for s in range(4):
-            t = ((place_ref[1] - s) & 3) * 2 + ((place_ref[2] + c) & 1)
+            t = ((x_ref[0] - s) & 3) * 2 + ((c_ref[0] + c) & 1)
             part = dot(features_ref[s].reshape(256, 768), value).astype(BF16).reshape(2, 4, 32, 128)
             for zz in range(2):
                 for y in range(4):
@@ -193,7 +198,7 @@
     rows = queries.shape[0]
     base = ((lax.axis_index("z") * 4 + lax.axis_index("y")) & 7) * 16
     base = base.astype(jnp.int32).reshape(1)
-    place = jnp.stack([lax.axis_index("y"), lax.axis_index("x"), lax.axis_index("c")]).astype(jnp.int32)
+    at_y, at_x, at_c = (lax.axis_index(axis).astype(jnp.int32).reshape(1) for axis in ("y", "x", "c"))
     (pieces,) = call(
         pack_kernel, [shape(1152, 128)], [SM, SM] + [VM] * 3, base, chosen, keys, values, normed, inputs=False
     )
@@ -202,7 +207,8 @@
     picked = exchange(picked.reshape(64, 16, 128), KV)
     (half,) = call(half_kernel, [shape(512, 128)], [VM], pieces)
     other = lax.ppermute(half, "y", [(n, n ^ 1) for n in range(4)])
-    (features,) = call(turn_kernel, [shape(2, 128, 768)], [SM] + [VM] * 3, place, half, other, normed)
+    (turned,) = call(turn_own_kernel, [shape(256, 256)], [VM], normed)
+    (features,) = call(turn_kernel, [shape(2, 128, 768)], [SM] + [VM] * 3, at_y, half, other, turned)
     parts = [features]
     for s in range(1, 4):
         parts.append(shift(features, "x", s))
@@ -219,8 +225,8 @@
     (sums,) = call(
         sum_kernel,
         [shape(4, 20, 32, 128)],
-        [SM] + [VM] * 5,
-        place, ids, back.reshape(1024, 128), own, features, others,
+        [SM] * 3 + [VM] * 5,
+        at_y, at_x, at_c, ids, back.reshape(1024, 128), own, features, others,
         limit=24,
     )
     sums = exchange(sums, "y")

time: 154 us -> 154 us (level)
  blocking collectives: 100 us -> 74.9 us
  waiting for transfers between devices: 19 us -> 38.9 us
  starting transfers between devices: 19.3 us -> 25 us
    all_to_all x4 -> x3, blocking collectives: 100 us -> 74.9 us  [exchange(): return lax.all_to_all(x, axis, split_axis=0, concat_axis=0, tiled=True)]
    all_to_all x1 -> x2, waiting for transfers between devices: 11.4 us -> 30.9 us  [exchange(): return lax.all_to_all(x, axis, split_axis=0, concat_axis=0, tiled=True)]
    all_to_all x1 -> x2, starting transfers between devices: 5.67 us -> 11.3 us  [exchange(): return lax.all_to_all(x, axis, split_axis=0, concat_axis=0, tiled=True)]
    pallas_call x8 -> x9, Pallas kernels: 11.8 us -> 11.4 us  [call(): pl.pallas_call(kernel, out_shape=[o if n in hbm else pltpu.VMEM(o.shape,...]
  transfers between devices with their start and end apart: 6 -> 7, of which waited for: 3 -> 4; matrix products, arithmetic and copies ran while one was open for 1% -> 1% of each run, Pallas kernels for 3% -> 3%
where the time goes in v1:
time: 154 us; the launch traced here: 153 us
  blocking collectives  74.9 us (49%)
  waiting for transfers between devices  38.9 us (25%)
  starting transfers between devices  25 us (16%)
  Pallas kernels  11.4 us (7%)
    all_to_all x3, blocking collectives, exchange(): return lax.all_to_all(x, axis, split_axis=0, concat_axis=0, tiled=True)  74.9 us
    all_to_all x2, waiting for transfers between devices, exchange(): return lax.all_to_all(x, axis, split_axis=0, concat_axis=0, tiled=True)  30.9 us
    pallas_call x9, Pallas kernels, call(): pl.pallas_call(kernel, out_shape=[o if n in hbm else pltpu.VMEM(o.shape,...  11.4 us
    all_to_all x2, starting transfers between devices, exchange(): return lax.all_to_all(x, axis, split_axis=0, concat_axis=0, tiled=True)  11.3 us
    ppermute x4, starting transfers between devices, shift(): return lax.ppermute(x, axis, [(n, (n + by) % size) for n in range(size)])  10.9 us
    ppermute x4, waiting for transfers between devices, shift(): return lax.ppermute(x, axis, [(n, (n + by) % size) for n in range(size)])  4.08 us
    ppermute x1, waiting for transfers between devices, body(): other = lax.ppermute(half, 'y', [(n, n ^ 1) for n in range(4)])  3.89 us
  transfers between devices with their start and end apart: 7, of which 4 were waited for; matrix products, arithmetic and copies ran while one was open for 1% of the time, Pallas kernels for 3%

profile of v1, /device:TPU:36, one launch (start us, length us, event | category | flops | bytes accessed | tf_op | source)
XLA Modules:
  0.0 153.0 jit_solution(13005307773810312530)
XLA Ops:
  0.6 0.0 copy-start
  0.6 1.8 %shard_map.102 = bf16[1152,128]{1,0:T(8,128)(2,1)S(1)} custom-call(s32[1]{0:T(128)} %bitcast.base_ref, s32[2,8]{1,0:T(2,128)} %chosen_ref.3, bf16[256,128]{1,0:T(8,128)(2,1)} %keys_ref.3, bf16[256,128]{1,0:T(8,128)(2,1)} %values_ref.3, bf16[256,256]{1,0:T(8,128)(2,1)} %normed_ref.3), custom_call_target="tpu_custom_call" | custom-call | tf_op jit(solution)/shard_map/pallas_call | solution.py:175
  2.5 41.3 %all_to_all.25 = bf16[64,9,2,128]{3,2,1,0:T(2,128)(2,1)S(1)} all-to-all(bf16[64,9,2,128]{3,2,1,0:T(2,128)(2,1)S(1)} %bitcast.17), channel_id=1, replica_groups=mesh['z'=16,'y'=4,'x'=4,'c'=2] {'z','y'}, dimensions={0} | all-to-all | bytes 589824 | tf_op jit(solution)/shard_map/all_to_all | solution.py:189
  43.8 0.5 shard_map.105.mine_ref
  44.3 2.7 %collective-permute-start = (bf16[512,128]{1,0:T(8,128)(2,1)S(1)}, bf16[512,128]{1,0:T(8,128)(2,1)S(1)}, u32[]{:S(2)}, u32[]{:S(2)}) collective-permute-start(bf16[512,128]{1,0:T(8,128)(2,1)S(1)} %shard_map.105.mine_ref), channel_id=1, source_target_pairs={{0,8},{8,0},{16,24},{24,16},{1,9},{9,1},{17,25},{25,17},{2,10},{10... | collective-permute-start | bytes 393224 | tf_op jit(solution)/shard_map/ppermute | solution.py:209
  47.0 0.0 copy-done
  47.0 0.2 shard_map.106.own_ref
  47.3 3.9 %collective-permute-done.other_ref = bf16[512,128]{1,0:T(8,128)(2,1)S(1)} collective-permute-done((bf16[512,128]{1,0:T(8,128)(2,1)S(1)}, bf16[512,128]{1,0:T(8,128)(2,1)S(1)}, u32[]{:S(2)}, u32[]{:S(2)}) %collective-permute-start) | collective-permute-done | bytes 131104 | tf_op jit(solution)/shard_map/ppermute | solution.py:209
  51.2 0.4 shard_map.107
  51.5 2.4 %collective-permute-start.3 = (bf16[2,128,768]{2,1,0:T(8,128)(2,1)S(1)}, bf16[2,128,768]{2,1,0:T(8,128)(2,1)S(1)}, u32[]{:S(2)}, u32[]{:S(2)}) collective-permute-start(bf16[2,128,768]{2,1,0:T(8,128)(2,1)S(1)} %shard_map.107), channel_id=1, source_target_pairs={{0,6},{2,0},{4,2},{6,4},{1,7},{3,1},{5,3},{7,5},{8,14},{10,8},{12,... | collective-permute-start | bytes 1179656 | tf_op jit(solution)/shard_map/ppermute | solution.py:194
  54.0 4.6 %collective-permute-start.2 = (bf16[2,128,768]{2,1,0:T(8,128)(2,1)S(1)}, bf16[2,128,768]{2,1,0:T(8,128)(2,1)S(1)}, u32[]{:S(2)}, u32[]{:S(2)}) collective-permute-start(bf16[2,128,768]{2,1,0:T(8,128)(2,1)S(1)} %shard_map.107), channel_id=1, source_target_pairs={{0,4},{2,6},{4,0},{6,2},{1,5},{3,7},{5,1},{7,3},{8,12},{10,14},{12... | collective-permute-start | bytes 1179656 | tf_op jit(solution)/shard_map/ppermute | solution.py:194
  58.6 1.9 %collective-permute-start.1 = (bf16[2,128,768]{2,1,0:T(8,128)(2,1)S(1)}, bf16[2,128,768]{2,1,0:T(8,128)(2,1)S(1)}, u32[]{:S(2)}, u32[]{:S(2)}) collective-permute-start(bf16[2,128,768]{2,1,0:T(8,128)(2,1)S(1)} %shard_map.107), channel_id=1, source_target_pairs={{0,2},{2,4},{4,6},{6,0},{1,3},{3,5},{5,7},{7,1},{8,10},{10,12},{12... | collective-permute-start | bytes 1179656 | tf_op jit(solution)/shard_map/ppermute | solution.py:194
  60.6 1.8 %shard_map.103 = (bf16[1024,128]{1,0:T(8,128)(2,1)}, f32[8,128]{1,0:T(8,128)S(1)}) custom-call(bf16[1152,128]{1,0:T(8,128)(2,1)S(1)} %bitcast.15), custom_call_target="tpu_custom_call" | custom-call | tf_op jit(solution)/shard_map/pallas_call | solution.py:175
  62.4 5.7 %all-to-all-start.1 = ((bf16[64,16,128]{2,1,0:T(8,128)(2,1)}), bf16[64,16,128]{2,1,0:T(8,128)(2,1)S(1)}, u32[]{:S(2)}, u32[]{:S(2)}) async-start(bf16[64,16,128]{2,1,0:T(8,128)(2,1)} %bitcast.3), calls=%async_computation.1 | async-start | bytes 524288 | tf_op jit(solution)/shard_map/all_to_all | solution.py:189
  68.0 0.0 collective-permute-done.3
  68.0 0.0 collective-permute-done.2
  68.1 4.1 %collective-permute-done.1 = bf16[2,128,768]{2,1,0:T(8,128)(2,1)S(1)} collective-permute-done((bf16[2,128,768]{2,1,0:T(8,128)(2,1)S(1)}, bf16[2,128,768]{2,1,0:T(8,128)(2,1)S(1)}, u32[]{:S(2)}, u32[]{:S(2)}) %collective-permute-start.1) | collective-permute-done | bytes 393248 | tf_op jit(solution)/shard_map/ppermute | solution.py:194
  72.1 0.0 copy-start.6
  72.1 0.8 copy-done.6
  72.9 0.0 copy-start.1
  72.9 0.0 copy-start.2
  72.9 0.0 copy-start.3
  72.9 0.0 copy-start.4
  72.9 0.0 copy-start.5
  72.9 1.2 pad_maximum_fusion.mine_ref
  74.1 1.9 %collective-permute-start.4 = (bf16[4,2,128,768]{3,2,1,0:T(8,128)(2,1)S(1)}, bf16[4,2,128,768]{3,2,1,0:T(8,128)(2,1)}, u32[]{:S(2)}, u32[]{:S(2)}) collective-permute-start(bf16[4,2,128,768]{3,2,1,0:T(8,128)(2,1)S(1)} %pad_maximum_fusion.mine_ref), channel_id=1, source_target_pairs={{0,1},{1,0},{2,3},{3,2},{4,5},{5,4},{6,7},{7,6},{8,9},{9,8},{10,11... | collective-permute-start | bytes 4718600 | tf_op jit(solution)/shard_map/ppermute | solution.py:194
  76.1 11.4 %all-to-all-done.1 = bf16[64,16,128]{2,1,0:T(8,128)(2,1)S(1)} async-done(((bf16[64,16,128]{2,1,0:T(8,128)(2,1)}), bf16[64,16,128]{2,1,0:T(8,128)(2,1)S(1)}, u32[]{:S(2)}, u32[]{:S(2)}) %all-to-all-start.1) | async-done | bytes 262176 | tf_op jit(solution)/shard_map/all_to_all | solution.py:189
  87.4 0.0 copy-done.1
  87.4 0.0 copy-done.2
  87.4 0.0 copy-done.3
  87.5 0.0 copy-done.4
  87.5 0.0 copy-done.5
  87.5 2.4 %shard_map.104 = (bf16[256,128]{1,0:T(8,128)(2,1)}, bf16[32,2,16,128]{3,2,1,0:T(8,128)(2,1)}, bf16[2,256,128]{2,1,0:T(8,128)(2,1)S(1)}) custom-call(s32[2,8]{1,0:T(2,128)} %chosen_ref.3, bf16[256,128]{1,0:T(8,128)(2,1)S(1)} %copy-done.3, bf16[256,128]{1,0:T(8,128)(2,1)S(1)} %copy-done.1, bf16[256,128]{1,0:T(8,128)(2,1)S(1)} %copy-done.2, ...), custom_call_target="tpu_custom_call" | custom-call | tf_op jit(solution)/shard_map/pallas_call | solution.py:175
  89.9 5.7 %all-to-all-start.2 = ((bf16[64,16,128]{2,1,0:T(8,128)(2,1)}), bf16[64,16,128]{2,1,0:T(8,128)(2,1)S(1)}, u32[]{:S(2)}, u32[]{:S(2)}) async-start(bf16[64,16,128]{2,1,0:T(8,128)(2,1)} %bitcast.8), calls=%async_computation.2 | async-start | bytes 524288 | tf_op jit(solution)/shard_map/all_to_all | solution.py:189
  95.6 19.6 %all-to-all-done.2 = bf16[64,16,128]{2,1,0:T(8,128)(2,1)S(1)} async-done(((bf16[64,16,128]{2,1,0:T(8,128)(2,1)}), bf16[64,16,128]{2,1,0:T(8,128)(2,1)S(1)}, u32[]{:S(2)}, u32[]{:S(2)}) %all-to-all-start.2) | async-done | bytes 262176 | tf_op jit(solution)/shard_map/all_to_all | solution.py:189
  115.1 0.0 collective-permute-done.4.other_ref
  115.1 3.2 %shard_map.108 = bf16[4,20,32,128]{3,2,1,0:T(8,128)(2,1)S(1)} custom-call(s32[1]{0:T(128)} %bitcast.5.y_ref, s32[1]{0:T(128)} %bitcast.6.x_ref, s32[1]{0:T(128)} %bitcast.7.c_ref, f32[8,128]{1,0:T(8,128)S(1)} %get-tuple-element.14.ids_ref, bf16[1024,128]{1,0:T(8,128)(2,1)S(1)} %bitcast.18, bf16[2,256,128]{2,1,0:T(8,128)(2,1)S(1)} %get-tuple-element.16.own_ref, ...), custom_call_target="tpu_custom_call" | custom-call | tf_op jit(solution)/shard_map/pallas_call | solution.py:175
  118.3 12.0 %all_to_all.26.got_ref = bf16[4,20,32,128]{3,2,1,0:T(8,128)(2,1)S(1)} all-to-all(bf16[4,20,32,128]{3,2,1,0:T(8,128)(2,1)S(1)} %shard_map.108), channel_id=1, replica_groups=mesh['z'=16,'y'=4,'x'=4,'c'=2] {'y'}, dimensions={0} | all-to-all | bytes 1310720 | tf_op jit(solution)/shard_map/all_to_all | solution.py:189
  130.3 0.1 shard_map.109
  130.4 21.6 %all_to_all.27.got_ref = bf16[16,64,128]{2,1,0:T(8,128)(2,1)S(1)} all-to-all(bf16[16,64,128]{2,1,0:T(8,128)(2,1)S(1)} %shard_map.109), channel_id=1, replica_groups=mesh['z'=16,'y'=4,'x'=4,'c'=2] {'z'}, dimensions={0} | all-to-all | bytes 524288 | tf_op jit(solution)/shard_map/all_to_all | solution.py:189
  152.0 1.0 shard_map.110
Async XLA Ops:
  0.6 46.4 %copy-start = (bf16[256,256]{1,0:T(8,128)(2,1)S(1)}, bf16[256,256]{1,0:T(8,128)(2,1)}, u32[]{:S(2)}) copy-start(bf16[256,256]{1,0:T(8,128)(2,1)} %normed_ref.3) | copy-start | bytes 393220
  44.3 6.9 %collective-permute-start = (bf16[512,128]{1,0:T(8,128)(2,1)S(1)}, bf16[512,128]{1,0:T(8,128)(2,1)S(1)}, u32[]{:S(2)}, u32[]{:S(2)}) collective-permute-start(bf16[512,128]{1,0:T(8,128)(2,1)S(1)} %shard_map.105.mine_ref), channel_id=1, source_target_pairs={{0,8},{8,0},{16,24},{24,16},{1,9},{9,1},{17,25},{25,17},{2,10},{10... | collective-permute-start | bytes 393224 | tf_op jit(solution)/shard_map/ppermute | solution.py:209
  51.5 16.5 %collective-permute-start.3 = (bf16[2,128,768]{2,1,0:T(8,128)(2,1)S(1)}, bf16[2,128,768]{2,1,0:T(8,128)(2,1)S(1)}, u32[]{:S(2)}, u32[]{:S(2)}) collective-permute-start(bf16[2,128,768]{2,1,0:T(8,128)(2,1)S(1)} %shard_map.107), channel_id=1, source_target_pairs={{0,6},{2,0},{4,2},{6,4},{1,7},{3,1},{5,3},{7,5},{8,14},{10,8},{12,... | collective-permute-start | bytes 1179656 | tf_op jit(solution)/shard_map/ppermute | solution.py:194
  54.0 14.1 %collective-permute-start.2 = (bf16[2,128,768]{2,1,0:T(8,128)(2,1)S(1)}, bf16[2,128,768]{2,1,0:T(8,128)(2,1)S(1)}, u32[]{:S(2)}, u32[]{:S(2)}) collective-permute-start(bf16[2,128,768]{2,1,0:T(8,128)(2,1)S(1)} %shard_map.107), channel_id=1, source_target_pairs={{0,4},{2,6},{4,0},{6,2},{1,5},{3,7},{5,1},{7,3},{8,12},{10,14},{12... | collective-permute-start | bytes 1179656 | tf_op jit(solution)/shard_map/ppermute | solution.py:194
  58.6 13.5 %collective-permute-start.1 = (bf16[2,128,768]{2,1,0:T(8,128)(2,1)S(1)}, bf16[2,128,768]{2,1,0:T(8,128)(2,1)S(1)}, u32[]{:S(2)}, u32[]{:S(2)}) collective-permute-start(bf16[2,128,768]{2,1,0:T(8,128)(2,1)S(1)} %shard_map.107), channel_id=1, source_target_pairs={{0,2},{2,4},{4,6},{6,0},{1,3},{3,5},{5,7},{7,1},{8,10},{10,12},{12... | collective-permute-start | bytes 1179656 | tf_op jit(solution)/shard_map/ppermute | solution.py:194
  62.4 25.1 %all-to-all-start.1 = ((bf16[64,16,128]{2,1,0:T(8,128)(2,1)}), bf16[64,16,128]{2,1,0:T(8,128)(2,1)S(1)}, u32[]{:S(2)}, u32[]{:S(2)}) async-start(bf16[64,16,128]{2,1,0:T(8,128)(2,1)} %bitcast.3), calls=%async_computation.1 | async-start | bytes 524288 | tf_op jit(solution)/shard_map/all_to_all | solution.py:189
  72.1 0.8 copy-start.6
  72.9 14.6 %copy-start.1 = (bf16[256,128]{1,0:T(8,128)(2,1)S(1)}, bf16[256,128]{1,0:T(8,128)(2,1)}, u32[]{:S(2)}) copy-start(bf16[256,128]{1,0:T(8,128)(2,1)} %keys_ref.3) | copy-start | bytes 196612
  72.9 14.6 %copy-start.2 = (bf16[256,128]{1,0:T(8,128)(2,1)S(1)}, bf16[256,128]{1,0:T(8,128)(2,1)}, u32[]{:S(2)}) copy-start(bf16[256,128]{1,0:T(8,128)(2,1)} %values_ref.3) | copy-start | bytes 196612
  72.9 14.6 %copy-start.3 = (bf16[256,128]{1,0:T(8,128)(2,1)S(1)}, bf16[256,128]{1,0:T(8,128)(2,1)}, u32[]{:S(2)}) copy-start(bf16[256,128]{1,0:T(8,128)(2,1)} %queries_ref.1) | copy-start | bytes 196612
  72.9 14.6 %copy-start.4 = (bf16[256,128]{1,0:T(8,128)(2,1)S(1)}, bf16[256,128]{1,0:T(8,128)(2,1)}, u32[]{:S(2)}) copy-start(bf16[256,128]{1,0:T(8,128)(2,1)} %grad_ref.1) | copy-start | bytes 196612
  72.9 14.6 %copy-start.5 = (f32[2,256]{1,0:T(2,128)S(1)}, f32[2,256]{1,0:T(2,128)}, u32[]{:S(2)}) copy-start(f32[2,256]{1,0:T(2,128)} %sums_ref.1) | copy-start | bytes 6148
  74.1 41.0 %collective-permute-start.4 = (bf16[4,2,128,768]{3,2,1,0:T(8,128)(2,1)S(1)}, bf16[4,2,128,768]{3,2,1,0:T(8,128)(2,1)}, u32[]{:S(2)}, u32[]{:S(2)}) collective-permute-start(bf16[4,2,128,768]{3,2,1,0:T(8,128)(2,1)S(1)} %pad_maximum_fusion.mine_ref), channel_id=1, source_target_pairs={{0,1},{1,0},{2,3},{3,2},{4,5},{5,4},{6,7},{7,6},{8,9},{9,8},{10,11... | collective-permute-start | bytes 4718600 | tf_op jit(solution)/shard_map/ppermute | solution.py:194
  89.9 25.2 %all-to-all-start.2 = ((bf16[64,16,128]{2,1,0:T(8,128)(2,1)}), bf16[64,16,128]{2,1,0:T(8,128)(2,1)S(1)}, u32[]{:S(2)}, u32[]{:S(2)}) async-start(bf16[64,16,128]{2,1,0:T(8,128)(2,1)} %bitcast.8), calls=%async_computation.2 | async-start | bytes 524288 | tf_op jit(solution)/shard_map/all_to_all | solution.py:189

commit v2 on v1

--- a/solution.py
+++ b/solution.py
@@ -67,22 +67,24 @@
         out_ref[j * 128 : (j + 1) * 128, :] = dot(hot, got).astype(BF16)
 
 
-def half_kernel(got_ref, out_ref):
+def half_kernel(y_ref, got_ref, normed_ref, mine_ref, sent_ref):
     row, col = iota((512, 64 * 18), 0), iota((512, 64 * 18), 1)
-    out_ref[...] = dot(one_hot(col == row + (row >> 3) * 10 + 10), got_ref[...]).astype(BF16)
-
-
-def turn_own_kernel(normed_ref, out_ref):
-    eye = one_hot(iota((256, 256), 0) == iota((256, 256), 1))
-    out_ref[...] = dot(normed_ref[...], eye, ((0,), (0,))).astype(BF16)
-
-
-def turn_kernel(y_ref, mine_ref, other_ref, own_ref, out_ref):
+    mine = dot(one_hot(col == row + (row >> 3) * 10 + 10), got_ref[...])
+    mine_ref[...] = mine.astype(BF16)
+    normed = normed_ref[...].astype(F32)
+    normed = jnp.concatenate([normed[:, :128], normed[:, 128:]], axis=0)
+    sent_ref[...] = jnp.where((y_ref[0] & 1) == 1, normed, mine).astype(BF16)
+
+
+def turn_kernel(y_ref, mine_ref, other_ref, normed_ref, out_ref):
     eye = one_hot(iota((512, 512), 0) == iota((512, 512), 1))
-    half = y_ref[0] & 1
-    out_ref[half, :, 256:] = dot(mine_ref[...], eye, ((0,), (0,))).astype(BF16)
-    out_ref[1 - half, :, 256:] = dot(other_ref[...], eye, ((0,), (0,))).astype(BF16)
-    out_ref[:, :, :256] = own_ref[...].reshape(2, 128, 256)
+    other = other_ref[...].astype(F32)
+    normed = normed_ref[...].astype(F32)
+    for n in range(2):
+        kept = other if n == 0 else mine_ref[...].astype(F32)
+        owned = jnp.concatenate([normed[:, n * 128 : (n + 1) * 128], other[n * 256 : (n + 1) * 256]], axis=0)
+        part = jnp.where((y_ref[0] & 1) == 1, kept, owned).astype(BF16)
+        out_ref[n] = dot(part, eye, ((0,), (0,))).astype(BF16)
 
 
 def attend_kernel(
@@ -127,18 +129,18 @@
         dq_ref[span, :] = (jnp.where(low_lanes, dq[:QB], dq[QB:]) * (HD**-0.5)).astype(BF16)
 
 
-def sum_kernel(y_ref, x_ref, c_ref, ids_ref, got_ref, own_ref, mine_ref, other_ref, out_ref):
+def sum_kernel(y_ref, x_ref, c_ref, ids_ref, got_ref, own_ref, partner_ref, mine_ref, other_ref, out_ref):
     number = (iota((512, 128), 0) + 1).astype(F32)
     sums = jnp.zeros((512, 128), F32)
     for j in range(8):
         hot = one_hot(number == ids_ref[j : j + 1, :])
         sums = sums + dot(hot, got_ref[j * 128 : (j + 1) * 128, :])
-    held = jnp.where((y_ref[0] & 1) == 1, sums, 0.0).astype(BF16)
-    value = jnp.concatenate([own_ref[1], held], axis=0)
+    owned = jnp.concatenate([own_ref[1], partner_ref[...]], axis=0).astype(F32)
+    value = jnp.where((y_ref[0] & 1) == 1, sums, owned).astype(BF16)
     for c, features_ref in enumerate((mine_ref, other_ref)):
         for s in range(4):
             t = ((x_ref[0] - s) & 3) * 2 + ((c_ref[0] + c) & 1)
-            part = dot(features_ref[s].reshape(256, 768), value).astype(BF16).reshape(2, 4, 32, 128)
+            part = dot(features_ref[s].reshape(256, 512), value).astype(BF16).reshape(2, 4, 32, 128)
             for zz in range(2):
                 for y in range(4):
                     out_ref[y, t * 2 + zz] = part[zz, y]
@@ -194,6 +196,10 @@
     return lax.ppermute(x, axis, [(n, (n + by) % size) for n in range(size)])
 
 
+def swapped(x):
+    return lax.ppermute(x, "y", [(n, n ^ 1) for n in range(4)])
+
+
 def body(queries, keys, values, log_sums, out_grad, chosen, normed):
     rows = queries.shape[0]
     base = ((lax.axis_index("z") * 4 + lax.axis_index("y")) & 7) * 16
@@ -205,10 +211,9 @@
     pieces = exchange(pieces.reshape(64, 9, 2, 128), KV).reshape(1152, 128)
     picked, ids = call(select_kernel, [shape(1024, 128), shape(8, 128, dtype=F32)], [VM], pieces)
     picked = exchange(picked.reshape(64, 16, 128), KV)
-    (half,) = call(half_kernel, [shape(512, 128)], [VM], pieces)
-    other = lax.ppermute(half, "y", [(n, n ^ 1) for n in range(4)])
-    (turned,) = call(turn_own_kernel, [shape(256, 256)], [VM], normed)
-    (features,) = call(turn_kernel, [shape(2, 128, 768)], [SM] + [VM] * 3, at_y, half, other, turned)
+    half, sent = call(half_kernel, [shape(512, 128)] * 2, [SM] + [VM] * 2, at_y, pieces, normed)
+    other = swapped(sent)
+    (features,) = call(turn_kernel, [shape(2, 128, 512)], [SM] + [VM] * 3, at_y, half, other, normed)
     parts = [features]
     for s in range(1, 4):
         parts.append(shift(features, "x", s))
@@ -222,11 +227,12 @@
         hbm=(0,),
     )
     back = exchange(back.reshape(64, 16, 128), KV)
+    partner = swapped(own[1])
     (sums,) = call(
         sum_kernel,
         [shape(4, 20, 32, 128)],
-        [SM] * 3 + [VM] * 5,
-        at_y, at_x, at_c, ids, back.reshape(1024, 128), own, features, others,
+        [SM] * 3 + [VM] * 6,
+        at_y, at_x, at_c, ids, back.reshape(1024, 128), own, partner, features, others,
         limit=24,
     )
     sums = exchange(sums, "y")

time: 154 us -> 159 us (1.032)
  the two profiles are of different devices: /device:TPU:36 before, /device:TPU:32 now
where the time goes in v2:
time: 159 us; the launch traced here: 158 us
  blocking collectives  76.1 us (48%)
  starting transfers between devices  39.9 us (25%)
  waiting for transfers between devices  31.7 us (20%)
  Pallas kernels  9.52 us (6%)
    all_to_all x3, blocking collectives, exchange(): return lax.all_to_all(x, axis, split_axis=0, concat_axis=0, tiled=True)  76.1 us
    all_to_all x2, starting transfers between devices, exchange(): return lax.all_to_all(x, axis, split_axis=0, concat_axis=0, tiled=True)  21 us
    all_to_all x2, waiting for transfers between devices, exchange(): return lax.all_to_all(x, axis, split_axis=0, concat_axis=0, tiled=True)  16.2 us
    ppermute x4, starting transfers between devices, shift(): return lax.ppermute(x, axis, [(n, (n + by) % size) for n in range(size)])  12.1 us
    pallas_call x8, Pallas kernels, call(): pl.pallas_call(kernel, out_shape=[o if n in hbm else pltpu.VMEM(o.shape,...  9.52 us
    ppermute x4, waiting for transfers between devices, shift(): return lax.ppermute(x, axis, [(n, (n + by) % size) for n in range(size)])  8.93 us
    ppermute x2, starting transfers between devices, swapped(): return lax.ppermute(x, 'y', [(n, n ^ 1) for n in range(4)])  6.74 us
    ppermute x2, waiting for transfers between devices, swapped(): return lax.ppermute(x, 'y', [(n, n ^ 1) for n in range(4)])  6.58 us
  transfers between devices with their start and end apart: 8, of which 6 were waited for; matrix products, arithmetic and copies ran while one was open for 0% of the time, Pallas kernels for 2%

profile of v2, /device:TPU:32, one launch (start us, length us, event | category | flops | bytes accessed | tf_op | source)
XLA Modules:
  0.0 158.2 jit_solution(1167181924368135067)
XLA Ops:
  0.6 1.8 %shard_map.102 = bf16[1152,128]{1,0:T(8,128)(2,1)S(1)} custom-call(s32[1]{0:T(128)} %bitcast.base_ref, s32[2,8]{1,0:T(2,128)} %chosen_ref.3, bf16[256,128]{1,0:T(8,128)(2,1)} %keys_ref.3, bf16[256,128]{1,0:T(8,128)(2,1)} %values_ref.3, bf16[256,256]{1,0:T(8,128)(2,1)} %normed_ref.5), custom_call_target="tpu_custom_call" | custom-call | tf_op jit(solution)/shard_map/pallas_call | solution.py:177
  2.5 41.3 %all_to_all.25 = bf16[64,9,2,128]{3,2,1,0:T(2,128)(2,1)S(1)} all-to-all(bf16[64,9,2,128]{3,2,1,0:T(2,128)(2,1)S(1)} %bitcast.18), channel_id=1, replica_groups=mesh['z'=16,'y'=4,'x'=4,'c'=2] {'z','y'}, dimensions={0} | all-to-all | bytes 589824 | tf_op jit(solution)/shard_map/all_to_all | solution.py:191
  43.8 1.8 %shard_map.103 = (bf16[1024,128]{1,0:T(8,128)(2,1)}, f32[8,128]{1,0:T(8,128)S(1)}) custom-call(bf16[1152,128]{1,0:T(8,128)(2,1)S(1)} %bitcast.16), custom_call_target="tpu_custom_call" | custom-call | tf_op jit(solution)/shard_map/pallas_call | solution.py:177
  45.6 0.0 copy-start
  45.6 5.8 %all-to-all-start.1 = ((bf16[64,16,128]{2,1,0:T(8,128)(2,1)}), bf16[64,16,128]{2,1,0:T(8,128)(2,1)S(1)}, u32[]{:S(2)}, u32[]{:S(2)}) async-start(bf16[64,16,128]{2,1,0:T(8,128)(2,1)} %bitcast.3), calls=%async_computation.1 | async-start | bytes 524288 | tf_op jit(solution)/shard_map/all_to_all | solution.py:191
  51.4 0.0 copy-done
  51.4 0.5 shard_map.105
  51.9 3.4 %collective-permute-start.1 = (bf16[512,128]{1,0:T(8,128)(2,1)S(1)}, bf16[512,128]{1,0:T(8,128)(2,1)S(1)}, u32[]{:S(2)}, u32[]{:S(2)}) collective-permute-start(bf16[512,128]{1,0:T(8,128)(2,1)S(1)} %get-tuple-element.20), channel_id=1, source_target_pairs={{0,8},{8,0},{16,24},{24,16},{1,9},{9,1},{17,25},{25,17},{2,10},{10... | collective-permute-start | bytes 393224 | tf_op jit(solution)/shard_map/ppermute | solution.py:200
  55.3 3.7 %collective-permute-done.1.other_ref = bf16[512,128]{1,0:T(8,128)(2,1)S(1)} collective-permute-done((bf16[512,128]{1,0:T(8,128)(2,1)S(1)}, bf16[512,128]{1,0:T(8,128)(2,1)S(1)}, u32[]{:S(2)}, u32[]{:S(2)}) %collective-permute-start.1) | collective-permute-done | bytes 131104 | tf_op jit(solution)/shard_map/ppermute | solution.py:200
  59.0 0.4 shard_map.106
  59.4 4.7 %collective-permute-start.4 = (bf16[2,128,512]{2,1,0:T(8,128)(2,1)S(1)}, bf16[2,128,512]{2,1,0:T(8,128)(2,1)S(1)}, u32[]{:S(2)}, u32[]{:S(2)}) collective-permute-start(bf16[2,128,512]{2,1,0:T(8,128)(2,1)S(1)} %shard_map.106), channel_id=1, source_target_pairs={{0,6},{2,0},{4,2},{6,4},{1,7},{3,1},{5,3},{7,5},{8,14},{10,8},{12,... | collective-permute-start | bytes 786440 | tf_op jit(solution)/shard_map/ppermute | solution.py:196
  64.1 2.7 %collective-permute-start.3 = (bf16[2,128,512]{2,1,0:T(8,128)(2,1)S(1)}, bf16[2,128,512]{2,1,0:T(8,128)(2,1)S(1)}, u32[]{:S(2)}, u32[]{:S(2)}) collective-permute-start(bf16[2,128,512]{2,1,0:T(8,128)(2,1)S(1)} %shard_map.106), channel_id=1, source_target_pairs={{0,4},{2,6},{4,0},{6,2},{1,5},{3,7},{5,1},{7,3},{8,12},{10,14},{12... | collective-permute-start | bytes 786440 | tf_op jit(solution)/shard_map/ppermute | solution.py:196
  66.8 2.8 %collective-permute-start.2 = (bf16[2,128,512]{2,1,0:T(8,128)(2,1)S(1)}, bf16[2,128,512]{2,1,0:T(8,128)(2,1)S(1)}, u32[]{:S(2)}, u32[]{:S(2)}) collective-permute-start(bf16[2,128,512]{2,1,0:T(8,128)(2,1)S(1)} %shard_map.106), channel_id=1, source_target_pairs={{0,2},{2,4},{4,6},{6,0},{1,3},{3,5},{5,7},{7,1},{8,10},{10,12},{12... | collective-permute-start | bytes 786440 | tf_op jit(solution)/shard_map/ppermute | solution.py:196
  69.6 3.6 %collective-permute-done.4 = bf16[2,128,512]{2,1,0:T(8,128)(2,1)S(1)} collective-permute-done((bf16[2,128,512]{2,1,0:T(8,128)(2,1)S(1)}, bf16[2,128,512]{2,1,0:T(8,128)(2,1)S(1)}, u32[]{:S(2)}, u32[]{:S(2)}) %collective-permute-start.4) | collective-permute-done | bytes 262176 | tf_op jit(solution)/shard_map/ppermute | solution.py:196
  73.2 2.5 %collective-permute-done.3 = bf16[2,128,512]{2,1,0:T(8,128)(2,1)S(1)} collective-permute-done((bf16[2,128,512]{2,1,0:T(8,128)(2,1)S(1)}, bf16[2,128,512]{2,1,0:T(8,128)(2,1)S(1)}, u32[]{:S(2)}, u32[]{:S(2)}) %collective-permute-start.3) | collective-permute-done | bytes 262176 | tf_op jit(solution)/shard_map/ppermute | solution.py:196
  75.7 2.8 %collective-permute-done.2 = bf16[2,128,512]{2,1,0:T(8,128)(2,1)S(1)} collective-permute-done((bf16[2,128,512]{2,1,0:T(8,128)(2,1)S(1)}, bf16[2,128,512]{2,1,0:T(8,128)(2,1)S(1)}, u32[]{:S(2)}, u32[]{:S(2)}) %collective-permute-start.2) | collective-permute-done | bytes 262176 | tf_op jit(solution)/shard_map/ppermute | solution.py:196
  78.5 0.0 copy-start.1
  78.5 0.0 copy-start.2
  78.5 0.0 copy-start.3
  78.5 0.0 copy-start.4
  78.5 0.0 copy-start.5
  78.5 0.1 pad_maximum_fusion.mine_ref
  78.7 1.9 %collective-permute-start.5 = (bf16[4,2,128,512]{3,2,1,0:T(8,128)(2,1)S(1)}, bf16[4,2,128,512]{3,2,1,0:T(8,128)(2,1)S(1)}, u32[]{:S(2)}, u32[]{:S(2)}) collective-permute-start(bf16[4,2,128,512]{3,2,1,0:T(8,128)(2,1)S(1)} %pad_maximum_fusion.mine_ref), channel_id=1, source_target_pairs={{0,1},{1,0},{2,3},{3,2},{4,5},{5,4},{6,7},{7,6},{8,9},{9,8},{10,11... | collective-permute-start | bytes 3145736 | tf_op jit(solution)/shard_map/ppermute | solution.py:196
  80.6 0.0 all-to-all-done.1
  80.6 0.0 copy-done.1
  80.6 0.0 copy-done.2
  80.6 0.0 copy-done.3
  80.6 0.0 copy-done.4
  80.7 0.0 copy-done.5
  80.7 2.4 %shard_map.104 = (bf16[256,128]{1,0:T(8,128)(2,1)}, bf16[32,2,16,128]{3,2,1,0:T(8,128)(2,1)}, bf16[2,256,128]{2,1,0:T(8,128)(2,1)S(1)}) custom-call(s32[2,8]{1,0:T(2,128)} %chosen_ref.3, bf16[256,128]{1,0:T(8,128)(2,1)S(1)} %copy-done.3, bf16[256,128]{1,0:T(8,128)(2,1)S(1)} %copy-done.1, bf16[256,128]{1,0:T(8,128)(2,1)S(1)} %copy-done.2, ...), custom_call_target="tpu_custom_call" | custom-call | tf_op jit(solution)/shard_map/pallas_call | solution.py:177
  83.1 15.2 %all-to-all-start.2 = ((bf16[64,16,128]{2,1,0:T(8,128)(2,1)}), bf16[64,16,128]{2,1,0:T(8,128)(2,1)S(1)}, u32[]{:S(2)}, u32[]{:S(2)}) async-start(bf16[64,16,128]{2,1,0:T(8,128)(2,1)} %bitcast.8), calls=%async_computation.2 | async-start | bytes 524288 | tf_op jit(solution)/shard_map/all_to_all | solution.py:191
  98.3 3.4 %collective-permute-start = (bf16[256,128]{1,0:T(8,128)(2,1)S(1)}, bf16[256,128]{1,0:T(8,128)(2,1)S(1)}, u32[]{:S(2)}, u32[]{:S(2)}) collective-permute-start(bf16[256,128]{1,0:T(8,128)(2,1)S(1)} %slice_bitcast_fusion), channel_id=1, source_target_pairs={{0,8},{8,0},{16,24},{24,16},{1,9},{9,1},{17,25},{25,17},{2,10},{10... | collective-permute-start | bytes 196616 | tf_op jit(solution)/shard_map/ppermute | solution.py:200
  101.7 2.9 %collective-permute-done.partner_ref = bf16[256,128]{1,0:T(8,128)(2,1)S(1)} collective-permute-done((bf16[256,128]{1,0:T(8,128)(2,1)S(1)}, bf16[256,128]{1,0:T(8,128)(2,1)S(1)}, u32[]{:S(2)}, u32[]{:S(2)}) %collective-permute-start) | collective-permute-done | bytes 65568 | tf_op jit(solution)/shard_map/ppermute | solution.py:200
  104.6 0.0 collective-permute-done.5.other_ref
  104.6 16.2 %all-to-all-done.2 = bf16[64,16,128]{2,1,0:T(8,128)(2,1)S(1)} async-done(((bf16[64,16,128]{2,1,0:T(8,128)(2,1)}), bf16[64,16,128]{2,1,0:T(8,128)(2,1)S(1)}, u32[]{:S(2)}, u32[]{:S(2)}) %all-to-all-start.2) | async-done | bytes 262176 | tf_op jit(solution)/shard_map/all_to_all | solution.py:191
  120.8 1.6 %shard_map.107 = bf16[4,20,32,128]{3,2,1,0:T(8,128)(2,1)S(1)} custom-call(s32[1]{0:T(128)} %bitcast.5.y_ref, s32[1]{0:T(128)} %bitcast.6.x_ref, s32[1]{0:T(128)} %bitcast.7.c_ref, f32[8,128]{1,0:T(8,128)S(1)} %get-tuple-element.16.ids_ref, bf16[1024,128]{1,0:T(8,128)(2,1)S(1)} %bitcast.19, bf16[2,256,128]{2,1,0:T(8,128)(2,1)S(1)} %get-tuple-element.18.own_ref, ...), custom_call_target="tpu_custom_call" | custom-call | tf_op jit(solution)/shard_map/pallas_call | solution.py:177
  122.4 12.0 %all_to_all.26.got_ref = bf16[4,20,32,128]{3,2,1,0:T(8,128)(2,1)S(1)} all-to-all(bf16[4,20,32,128]{3,2,1,0:T(8,128)(2,1)S(1)} %shard_map.107), channel_id=1, replica_groups=mesh['z'=16,'y'=4,'x'=4,'c'=2] {'y'}, dimensions={0} | all-to-all | bytes 1310720 | tf_op jit(solution)/shard_map/all_to_all | solution.py:191
  134.4 0.1 shard_map.108
  134.5 22.8 %all_to_all.27.got_ref = bf16[16,64,128]{2,1,0:T(8,128)(2,1)S(1)} all-to-all(bf16[16,64,128]{2,1,0:T(8,128)(2,1)S(1)} %shard_map.108), channel_id=1, replica_groups=mesh['z'=16,'y'=4,'x'=4,'c'=2] {'z'}, dimensions={0} | all-to-all | bytes 524288 | tf_op jit(solution)/shard_map/all_to_all | solution.py:191
  157.2 1.0 shard_map.109
  (1 shorter events, 0.0 us)
Async XLA Ops:
  45.6 5.8 %copy-start = (bf16[256,256]{1,0:T(8,128)(2,1)S(1)}, bf16[256,256]{1,0:T(8,128)(2,1)}, u32[]{:S(2)}) copy-start(bf16[256,256]{1,0:T(8,128)(2,1)} %normed_ref.5) | copy-start | bytes 393220
  45.6 35.0 %all-to-all-start.1 = ((bf16[64,16,128]{2,1,0:T(8,128)(2,1)}), bf16[64,16,128]{2,1,0:T(8,128)(2,1)S(1)}, u32[]{:S(2)}, u32[]{:S(2)}) async-start(bf16[64,16,128]{2,1,0:T(8,128)(2,1)} %bitcast.3), calls=%async_computation.1 | async-start | bytes 524288 | tf_op jit(solution)/shard_map/all_to_all | solution.py:191
  51.9 7.1 %collective-permute-start.1 = (bf16[512,128]{1,0:T(8,128)(2,1)S(1)}, bf16[512,128]{1,0:T(8,128)(2,1)S(1)}, u32[]{:S(2)}, u32[]{:S(2)}) collective-permute-start(bf16[512,128]{1,0:T(8,128)(2,1)S(1)} %get-tuple-element.20), channel_id=1, source_target_pairs={{0,8},{8,0},{16,24},{24,16},{1,9},{9,1},{17,25},{25,17},{2,10},{10... | collective-permute-start | bytes 393224 | tf_op jit(solution)/shard_map/ppermute | solution.py:200
  59.4 13.8 %collective-permute-start.4 = (bf16[2,128,512]{2,1,0:T(8,128)(2,1)S(1)}, bf16[2,128,512]{2,1,0:T(8,128)(2,1)S(1)}, u32[]{:S(2)}, u32[]{:S(2)}) collective-permute-start(bf16[2,128,512]{2,1,0:T(8,128)(2,1)S(1)} %shard_map.106), channel_id=1, source_target_pairs={{0,6},{2,0},{4,2},{6,4},{1,7},{3,1},{5,3},{7,5},{8,14},{10,8},{12,... | collective-permute-start | bytes 786440 | tf_op jit(solution)/shard_map/ppermute | solution.py:196
  64.1 11.6 %collective-permute-start.3 = (bf16[2,128,512]{2,1,0:T(8,128)(2,1)S(1)}, bf16[2,128,512]{2,1,0:T(8,128)(2,1)S(1)}, u32[]{:S(2)}, u32[]{:S(2)}) collective-permute-start(bf16[2,128,512]{2,1,0:T(8,128)(2,1)S(1)} %shard_map.106), channel_id=1, source_target_pairs={{0,4},{2,6},{4,0},{6,2},{1,5},{3,7},{5,1},{7,3},{8,12},{10,14},{12... | collective-permute-start | bytes 786440 | tf_op jit(solution)/shard_map/ppermute | solution.py:196
  66.8 11.7 %collective-permute-start.2 = (bf16[2,128,512]{2,1,0:T(8,128)(2,1)S(1)}, bf16[2,128,512]{2,1,0:T(8,128)(2,1)S(1)}, u32[]{:S(2)}, u32[]{:S(2)}) collective-permute-start(bf16[2,128,512]{2,1,0:T(8,128)(2,1)S(1)} %shard_map.106), channel_id=1, source_target_pairs={{0,2},{2,4},{4,6},{6,0},{1,3},{3,5},{5,7},{7,1},{8,10},{10,12},{12... | collective-permute-start | bytes 786440 | tf_op jit(solution)/shard_map/ppermute | solution.py:196
  78.5 2.1 %copy-start.1 = (bf16[256,128]{1,0:T(8,128)(2,1)S(1)}, bf16[256,128]{1,0:T(8,128)(2,1)}, u32[]{:S(2)}) copy-start(bf16[256,128]{1,0:T(8,128)(2,1)} %keys_ref.3) | copy-start | bytes 196612
  78.5 2.1 %copy-start.2 = (bf16[256,128]{1,0:T(8,128)(2,1)S(1)}, bf16[256,128]{1,0:T(8,128)(2,1)}, u32[]{:S(2)}) copy-start(bf16[256,128]{1,0:T(8,128)(2,1)} %values_ref.3) | copy-start | bytes 196612
  78.5 2.1 %copy-start.3 = (bf16[256,128]{1,0:T(8,128)(2,1)S(1)}, bf16[256,128]{1,0:T(8,128)(2,1)}, u32[]{:S(2)}) copy-start(bf16[256,128]{1,0:T(8,128)(2,1)} %queries_ref.1) | copy-start | bytes 196612
  78.5 2.1 %copy-start.4 = (bf16[256,128]{1,0:T(8,128)(2,1)S(1)}, bf16[256,128]{1,0:T(8,128)(2,1)}, u32[]{:S(2)}) copy-start(bf16[256,128]{1,0:T(8,128)(2,1)} %grad_ref.1) | copy-start | bytes 196612
  78.5 2.1 %copy-start.5 = (f32[2,256]{1,0:T(2,128)S(1)}, f32[2,256]{1,0:T(2,128)}, u32[]{:S(2)}) copy-start(f32[2,256]{1,0:T(2,128)} %sums_ref.1) | copy-start | bytes 6148
  78.7 25.9 %collective-permute-start.5 = (bf16[4,2,128,512]{3,2,1,0:T(8,128)(2,1)S(1)}, bf16[4,2,128,512]{3,2,1,0:T(8,128)(2,1)S(1)}, u32[]{:S(2)}, u32[]{:S(2)}) collective-permute-start(bf16[4,2,128,512]{3,2,1,0:T(8,128)(2,1)S(1)} %pad_maximum_fusion.mine_ref), channel_id=1, source_target_pairs={{0,1},{1,0},{2,3},{3,2},{4,5},{5,4},{6,7},{7,6},{8,9},{9,8},{10,11... | collective-permute-start | bytes 3145736 | tf_op jit(solution)/shard_map/ppermute | solution.py:196
  83.1 37.7 %all-to-all-start.2 = ((bf16[64,16,128]{2,1,0:T(8,128)(2,1)}), bf16[64,16,128]{2,1,0:T(8,128)(2,1)S(1)}, u32[]{:S(2)}, u32[]{:S(2)}) async-start(bf16[64,16,128]{2,1,0:T(8,128)(2,1)} %bitcast.8), calls=%async_computation.2 | async-start | bytes 524288 | tf_op jit(solution)/shard_map/all_to_all | solution.py:191
  98.3 6.2 %collective-permute-start = (bf16[256,128]{1,0:T(8,128)(2,1)S(1)}, bf16[256,128]{1,0:T(8,128)(2,1)S(1)}, u32[]{:S(2)}, u32[]{:S(2)}) collective-permute-start(bf16[256,128]{1,0:T(8,128)(2,1)S(1)} %slice_bitcast_fusion), channel_id=1, source_target_pairs={{0,8},{8,0},{16,24},{24,16},{1,9},{9,1},{17,25},{25,17},{2,10},{10... | collective-permute-start | bytes 196616 | tf_op jit(solution)/shard_map/ppermute | solution.py:200

commit v3 on v2

--- a/solution.py
+++ b/solution.py
@@ -52,28 +52,25 @@
     out_ref[...] = (jnp.where((piece & 1) == 0, both[:, :128], both[:, 128:]) + extra).astype(BF16)
 
 
-def select_kernel(got_ref, out_ref, ids_ref):
+def select_kernel(got_ref, meta_ref, out_ref, ids_ref):
     got = got_ref[...]
-    group, col = iota((8, 64 * 18), 0) * 144, iota((8, 64 * 18), 1)
-    kind = col - ((col * 3641) >> 16) * 18
-    inside = (col >= group) & (col < group + 144)
-    ids = dot(one_hot(inside & (kind == 8)), got) * 8.0 + dot(one_hot(inside & (kind == 9)), got)
+    meta = meta_ref[...]
+    group, col = iota((8, 128), 0) * 16, iota((8, 128), 1)
+    inside = (col >= group) & (col < group + 16)
+    even = (col & 1) == 0
+    ids = dot(one_hot(inside & even), meta) * 8.0 + dot(one_hot(inside & ~even), meta)
     ids_ref[...] = ids
-    entry = ids.astype(jnp.int32) - 1
-    columns = jnp.where(entry >= 0, entry + (entry >> 3) * 10, -1).astype(F32).T
-    number = iota((128, 64 * 18), 1).astype(F32)
+    columns = ids.T
+    number = (iota((128, 512), 1) + 1).astype(F32)
     for j in range(8):
         hot = one_hot(number == columns[:, j : j + 1])
         out_ref[j * 128 : (j + 1) * 128, :] = dot(hot, got).astype(BF16)
 
 
-def half_kernel(y_ref, got_ref, normed_ref, mine_ref, sent_ref):
-    row, col = iota((512, 64 * 18), 0), iota((512, 64 * 18), 1)
-    mine = dot(one_hot(col == row + (row >> 3) * 10 + 10), got_ref[...])
-    mine_ref[...] = mine.astype(BF16)
+def sent_kernel(y_ref, ids_ref, mine_ref, normed_ref, out_ref):
     normed = normed_ref[...].astype(F32)
     normed = jnp.concatenate([normed[:, :128], normed[:, 128:]], axis=0)
-    sent_ref[...] = jnp.where((y_ref[0] & 1) == 1, normed, mine).astype(BF16)
+    out_ref[...] = jnp.where((y_ref[0] & 1) == 1, normed, mine_ref[...].astype(F32)).astype(BF16)
 
 
 def turn_kernel(y_ref, mine_ref, other_ref, normed_ref, out_ref):
@@ -98,8 +95,7 @@
         span = slice(g * QB, (g + 1) * QB)
         picked = []
         for n in range(2):
-            got = got_ref[:, n].astype(F32)[:, g * SEL : (g + 1) * SEL, :]
-            picked.append(got.reshape(KB * SEL, 128).astype(BF16))
+            picked.append(got_ref[:, n, g * SEL : (g + 1) * SEL, :].reshape(KB * SEL, 128))
         keys = jnp.concatenate([picked[0], keys_ref[span, :]], axis=0)
         values = jnp.concatenate([picked[1], values_ref[span, :]], axis=0)
         q = queries_ref[span, :].astype(F32) * (HD**-0.5)
@@ -208,10 +204,11 @@
     (pieces,) = call(
         pack_kernel, [shape(1152, 128)], [SM, SM] + [VM] * 3, base, chosen, keys, values, normed, inputs=False
     )
-    pieces = exchange(pieces.reshape(64, 9, 2, 128), KV).reshape(1152, 128)
-    picked, ids = call(select_kernel, [shape(1024, 128), shape(8, 128, dtype=F32)], [VM], pieces)
+    pieces = exchange(pieces.reshape(64, 9, 2, 128), KV)
+    table, meta, half = (pieces[:, a:b].reshape(-1, 128) for a, b in ((0, 4), (4, 5), (5, 9)))
+    picked, ids = call(select_kernel, [shape(1024, 128), shape(8, 128, dtype=F32)], [VM] * 2, table, meta)
     picked = exchange(picked.reshape(64, 16, 128), KV)
-    half, sent = call(half_kernel, [shape(512, 128)] * 2, [SM] + [VM] * 2, at_y, pieces, normed)
+    (sent,) = call(sent_kernel, [shape(512, 128)], [SM] + [VM] * 3, at_y, ids, half, normed)
     other = swapped(sent)
     (features,) = call(turn_kernel, [shape(2, 128, 512)], [SM] + [VM] * 3, at_y, half, other, normed)
     parts = [features]

time: 159 us -> 158 us (level)
  no operation moved by 1% of the time
where the time goes in v3:
time: 158 us
  blocking collectives  76.1 us (48%)
  starting transfers between devices  39.7 us (25%)
  waiting for transfers between devices  31.9 us (20%)
  Pallas kernels  8.66 us (5%)
    all_to_all x3, blocking collectives, exchange(): return lax.all_to_all(x, axis, split_axis=0, concat_axis=0, tiled=True)  76.1 us
    all_to_all x2, starting transfers between devices, exchange(): return lax.all_to_all(x, axis, split_axis=0, concat_axis=0, tiled=True)  20.9 us
    all_to_all x2, waiting for transfers between devices, exchange(): return lax.all_to_all(x, axis, split_axis=0, concat_axis=0, tiled=True)  16.2 us
    ppermute x4, starting transfers between devices, shift(): return lax.ppermute(x, axis, [(n, (n + by) % size) for n in range(size)])  12.1 us
    ppermute x4, waiting for transfers between devices, shift(): return lax.ppermute(x, axis, [(n, (n + by) % size) for n in range(size)])  8.99 us
    pallas_call x8, Pallas kernels, call(): pl.pallas_call(kernel, out_shape=[o if n in hbm else pltpu.VMEM(o.shape,...  8.66 us
    ppermute x2, starting transfers between devices, swapped(): return lax.ppermute(x, 'y', [(n, n ^ 1) for n in range(4)])  6.74 us
    ppermute x2, waiting for transfers between devices, swapped(): return lax.ppermute(x, 'y', [(n, n ^ 1) for n in range(4)])  6.65 us
  transfers between devices with their start and end apart: 8, of which 6 were waited for; matrix products, arithmetic and copies ran while one was open for 0% of the time, Pallas kernels for 2%

profile of v3, /device:TPU:32, one launch (start us, length us, event | category | flops | bytes accessed | tf_op | source)
XLA Modules:
  0.0 157.5 jit_solution(3141086716345349358)
XLA Ops:
  0.6 1.8 %shard_map.102 = bf16[1152,128]{1,0:T(8,128)(2,1)S(1)} custom-call(s32[1]{0:T(128)} %bitcast.base_ref, s32[2,8]{1,0:T(2,128)} %chosen_ref.3, bf16[256,128]{1,0:T(8,128)(2,1)} %keys_ref.3, bf16[256,128]{1,0:T(8,128)(2,1)} %values_ref.3, bf16[256,256]{1,0:T(8,128)(2,1)} %normed_ref.5), custom_call_target="tpu_custom_call" | custom-call | tf_op jit(solution)/shard_map/pallas_call | solution.py:173
  2.5 41.3 %all_to_all.25 = bf16[64,9,2,128]{3,2,1,0:T(2,128)(2,1)S(1)} all-to-all(bf16[64,9,2,128]{3,2,1,0:T(2,128)(2,1)S(1)} %bitcast.18), channel_id=1, replica_groups=mesh['z'=16,'y'=4,'x'=4,'c'=2] {'z','y'}, dimensions={0} | all-to-all | bytes 589824 | tf_op jit(solution)/shard_map/all_to_all | solution.py:187
  43.8 0.2 fusion
  44.0 1.4 shard_map.103
  45.4 0.0 copy-start
  45.4 5.8 %all-to-all-start.1 = ((bf16[64,16,128]{2,1,0:T(8,128)(2,1)}), bf16[64,16,128]{2,1,0:T(8,128)(2,1)S(1)}, u32[]{:S(2)}, u32[]{:S(2)}) async-start(bf16[64,16,128]{2,1,0:T(8,128)(2,1)} %bitcast.4), calls=%async_computation.1 | async-start | bytes 524288 | tf_op jit(solution)/shard_map/all_to_all | solution.py:187
  51.2 0.0 copy-done
  51.3 3.4 %collective-permute-start.1 = (bf16[512,128]{1,0:T(8,128)(2,1)S(1)}, bf16[512,128]{1,0:T(8,128)(2,1)S(1)}, u32[]{:S(2)}, u32[]{:S(2)}) collective-permute-start(bf16[512,128]{1,0:T(8,128)(2,1)S(1)} %shard_map.105), channel_id=1, source_target_pairs={{0,8},{8,0},{16,24},{24,16},{1,9},{9,1},{17,25},{25,17},{2,10},{10... | collective-permute-start | bytes 393224 | tf_op jit(solution)/shard_map/ppermute | solution.py:196
  54.6 3.8 %collective-permute-done.1.other_ref = bf16[512,128]{1,0:T(8,128)(2,1)S(1)} collective-permute-done((bf16[512,128]{1,0:T(8,128)(2,1)S(1)}, bf16[512,128]{1,0:T(8,128)(2,1)S(1)}, u32[]{:S(2)}, u32[]{:S(2)}) %collective-permute-start.1) | collective-permute-done | bytes 131104 | tf_op jit(solution)/shard_map/ppermute | solution.py:196
  58.4 0.4 shard_map.106
  58.8 4.7 %collective-permute-start.4 = (bf16[2,128,512]{2,1,0:T(8,128)(2,1)S(1)}, bf16[2,128,512]{2,1,0:T(8,128)(2,1)S(1)}, u32[]{:S(2)}, u32[]{:S(2)}) collective-permute-start(bf16[2,128,512]{2,1,0:T(8,128)(2,1)S(1)} %shard_map.106), channel_id=1, source_target_pairs={{0,6},{2,0},{4,2},{6,4},{1,7},{3,1},{5,3},{7,5},{8,14},{10,8},{12,... | collective-permute-start | bytes 786440 | tf_op jit(solution)/shard_map/ppermute | solution.py:192
  63.5 2.7 %collective-permute-start.3 = (bf16[2,128,512]{2,1,0:T(8,128)(2,1)S(1)}, bf16[2,128,512]{2,1,0:T(8,128)(2,1)S(1)}, u32[]{:S(2)}, u32[]{:S(2)}) collective-permute-start(bf16[2,128,512]{2,1,0:T(8,128)(2,1)S(1)} %shard_map.106), channel_id=1, source_target_pairs={{0,4},{2,6},{4,0},{6,2},{1,5},{3,7},{5,1},{7,3},{8,12},{10,14},{12... | collective-permute-start | bytes 786440 | tf_op jit(solution)/shard_map/ppermute | solution.py:192
  66.2 2.8 %collective-permute-start.2 = (bf16[2,128,512]{2,1,0:T(8,128)(2,1)S(1)}, bf16[2,128,512]{2,1,0:T(8,128)(2,1)S(1)}, u32[]{:S(2)}, u32[]{:S(2)}) collective-permute-start(bf16[2,128,512]{2,1,0:T(8,128)(2,1)S(1)} %shard_map.106), channel_id=1, source_target_pairs={{0,2},{2,4},{4,6},{6,0},{1,3},{3,5},{5,7},{7,1},{8,10},{10,12},{12... | collective-permute-start | bytes 786440 | tf_op jit(solution)/shard_map/ppermute | solution.py:192
  69.0 3.7 %collective-permute-done.4 = bf16[2,128,512]{2,1,0:T(8,128)(2,1)S(1)} collective-permute-done((bf16[2,128,512]{2,1,0:T(8,128)(2,1)S(1)}, bf16[2,128,512]{2,1,0:T(8,128)(2,1)S(1)}, u32[]{:S(2)}, u32[]{:S(2)}) %collective-permute-start.4) | collective-permute-done | bytes 262176 | tf_op jit(solution)/shard_map/ppermute | solution.py:192
  72.7 2.5 %collective-permute-done.3 = bf16[2,128,512]{2,1,0:T(8,128)(2,1)S(1)} collective-permute-done((bf16[2,128,512]{2,1,0:T(8,128)(2,1)S(1)}, bf16[2,128,512]{2,1,0:T(8,128)(2,1)S(1)}, u32[]{:S(2)}, u32[]{:S(2)}) %collective-permute-start.3) | collective-permute-done | bytes 262176 | tf_op jit(solution)/shard_map/ppermute | solution.py:192
  75.2 2.8 %collective-permute-done.2 = bf16[2,128,512]{2,1,0:T(8,128)(2,1)S(1)} collective-permute-done((bf16[2,128,512]{2,1,0:T(8,128)(2,1)S(1)}, bf16[2,128,512]{2,1,0:T(8,128)(2,1)S(1)}, u32[]{:S(2)}, u32[]{:S(2)}) %collective-permute-start.2) | collective-permute-done | bytes 262176 | tf_op jit(solution)/shard_map/ppermute | solution.py:192
  78.0 0.0 copy-start.1
  78.0 0.0 copy-start.2
  78.0 0.0 copy-start.3
  78.0 0.0 copy-start.4
  78.0 0.0 copy-start.5
  78.0 0.1 pad_maximum_fusion.mine_ref
  78.2 1.9 %collective-permute-start.5 = (bf16[4,2,128,512]{3,2,1,0:T(8,128)(2,1)S(1)}, bf16[4,2,128,512]{3,2,1,0:T(8,128)(2,1)S(1)}, u32[]{:S(2)}, u32[]{:S(2)}) collective-permute-start(bf16[4,2,128,512]{3,2,1,0:T(8,128)(2,1)S(1)} %pad_maximum_fusion.mine_ref), channel_id=1, source_target_pairs={{0,1},{1,0},{2,3},{3,2},{4,5},{5,4},{6,7},{7,6},{8,9},{9,8},{10,11... | collective-permute-start | bytes 3145736 | tf_op jit(solution)/shard_map/ppermute | solution.py:192
  80.1 0.0 all-to-all-done.1
  80.1 0.0 copy-done.1
  80.1 0.0 copy-done.2
  80.1 0.0 copy-done.3
  80.1 0.0 copy-done.4
  80.1 0.0 copy-done.5
  80.2 2.4 %shard_map.104 = (bf16[256,128]{1,0:T(8,128)(2,1)}, bf16[32,2,16,128]{3,2,1,0:T(8,128)(2,1)}, bf16[2,256,128]{2,1,0:T(8,128)(2,1)S(1)}) custom-call(s32[2,8]{1,0:T(2,128)} %chosen_ref.3, bf16[256,128]{1,0:T(8,128)(2,1)S(1)} %copy-done.3, bf16[256,128]{1,0:T(8,128)(2,1)S(1)} %copy-done.1, bf16[256,128]{1,0:T(8,128)(2,1)S(1)} %copy-done.2, ...), custom_call_target="tpu_custom_call" | custom-call | tf_op jit(solution)/shard_map/pallas_call | solution.py:173
  82.5 15.1 %all-to-all-start.2 = ((bf16[64,16,128]{2,1,0:T(8,128)(2,1)}), bf16[64,16,128]{2,1,0:T(8,128)(2,1)S(1)}, u32[]{:S(2)}, u32[]{:S(2)}) async-start(bf16[64,16,128]{2,1,0:T(8,128)(2,1)} %bitcast.9), calls=%async_computation.2 | async-start | bytes 524288 | tf_op jit(solution)/shard_map/all_to_all | solution.py:187
  97.6 3.4 %collective-permute-start = (bf16[256,128]{1,0:T(8,128)(2,1)S(1)}, bf16[256,128]{1,0:T(8,128)(2,1)S(1)}, u32[]{:S(2)}, u32[]{:S(2)}) collective-permute-start(bf16[256,128]{1,0:T(8,128)(2,1)S(1)} %slice_bitcast_fusion), channel_id=1, source_target_pairs={{0,8},{8,0},{16,24},{24,16},{1,9},{9,1},{17,25},{25,17},{2,10},{10... | collective-permute-start | bytes 196616 | tf_op jit(solution)/shard_map/ppermute | solution.py:196
  101.0 2.9 %collective-permute-done.partner_ref = bf16[256,128]{1,0:T(8,128)(2,1)S(1)} collective-permute-done((bf16[256,128]{1,0:T(8,128)(2,1)S(1)}, bf16[256,128]{1,0:T(8,128)(2,1)S(1)}, u32[]{:S(2)}, u32[]{:S(2)}) %collective-permute-start) | collective-permute-done | bytes 65568 | tf_op jit(solution)/shard_map/ppermute | solution.py:196
  103.9 0.0 collective-permute-done.5.other_ref
  103.9 16.2 %all-to-all-done.2 = bf16[64,16,128]{2,1,0:T(8,128)(2,1)S(1)} async-done(((bf16[64,16,128]{2,1,0:T(8,128)(2,1)}), bf16[64,16,128]{2,1,0:T(8,128)(2,1)S(1)}, u32[]{:S(2)}, u32[]{:S(2)}) %all-to-all-start.2) | async-done | bytes 262176 | tf_op jit(solution)/shard_map/all_to_all | solution.py:187
  120.1 1.6 %shard_map.107 = bf16[4,20,32,128]{3,2,1,0:T(8,128)(2,1)S(1)} custom-call(s32[1]{0:T(128)} %bitcast.6.y_ref, s32[1]{0:T(128)} %bitcast.7.x_ref, s32[1]{0:T(128)} %bitcast.8.c_ref, f32[8,128]{1,0:T(8,128)S(1)} %get-tuple-element.14.ids_ref, bf16[1024,128]{1,0:T(8,128)(2,1)S(1)} %bitcast.21, bf16[2,256,128]{2,1,0:T(8,128)(2,1)S(1)} %get-tuple-element.16.own_ref, ...), custom_call_target="tpu_custom_call" | custom-call | tf_op jit(solution)/shard_map/pallas_call | solution.py:173
  121.7 12.0 %all_to_all.26.got_ref = bf16[4,20,32,128]{3,2,1,0:T(8,128)(2,1)S(1)} all-to-all(bf16[4,20,32,128]{3,2,1,0:T(8,128)(2,1)S(1)} %shard_map.107), channel_id=1, replica_groups=mesh['z'=16,'y'=4,'x'=4,'c'=2] {'y'}, dimensions={0} | all-to-all | bytes 1310720 | tf_op jit(solution)/shard_map/all_to_all | solution.py:187
  133.7 0.1 shard_map.108
  133.8 22.8 %all_to_all.27.got_ref = bf16[16,64,128]{2,1,0:T(8,128)(2,1)S(1)} all-to-all(bf16[16,64,128]{2,1,0:T(8,128)(2,1)S(1)} %shard_map.108), channel_id=1, replica_groups=mesh['z'=16,'y'=4,'x'=4,'c'=2] {'z'}, dimensions={0} | all-to-all | bytes 524288 | tf_op jit(solution)/shard_map/all_to_all | solution.py:187
  156.6 1.0 shard_map.109
  (3 shorter events, 0.1 us)
Async XLA Ops:
  45.4 5.8 %copy-start = (bf16[256,256]{1,0:T(8,128)(2,1)S(1)}, bf16[256,256]{1,0:T(8,128)(2,1)}, u32[]{:S(2)}) copy-start(bf16[256,256]{1,0:T(8,128)(2,1)} %normed_ref.5) | copy-start | bytes 393220
  45.4 34.7 %all-to-all-start.1 = ((bf16[64,16,128]{2,1,0:T(8,128)(2,1)}), bf16[64,16,128]{2,1,0:T(8,128)(2,1)S(1)}, u32[]{:S(2)}, u32[]{:S(2)}) async-start(bf16[64,16,128]{2,1,0:T(8,128)(2,1)} %bitcast.4), calls=%async_computation.1 | async-start | bytes 524288 | tf_op jit(solution)/shard_map/all_to_all | solution.py:187
  51.3 7.2 %collective-permute-start.1 = (bf16[512,128]{1,0:T(8,128)(2,1)S(1)}, bf16[512,128]{1,0:T(8,128)(2,1)S(1)}, u32[]{:S(2)}, u32[]{:S(2)}) collective-permute-start(bf16[512,128]{1,0:T(8,128)(2,1)S(1)} %shard_map.105), channel_id=1, source_target_pairs={{0,8},{8,0},{16,24},{24,16},{1,9},{9,1},{17,25},{25,17},{2,10},{10... | collective-permute-start | bytes 393224 | tf_op jit(solution)/shard_map/ppermute | solution.py:196
  58.8 13.9 %collective-permute-start.4 = (bf16[2,128,512]{2,1,0:T(8,128)(2,1)S(1)}, bf16[2,128,512]{2,1,0:T(8,128)(2,1)S(1)}, u32[]{:S(2)}, u32[]{:S(2)}) collective-permute-start(bf16[2,128,512]{2,1,0:T(8,128)(2,1)S(1)} %shard_map.106), channel_id=1, source_target_pairs={{0,6},{2,0},{4,2},{6,4},{1,7},{3,1},{5,3},{7,5},{8,14},{10,8},{12,... | collective-permute-start | bytes 786440 | tf_op jit(solution)/shard_map/ppermute | solution.py:192
  63.5 11.7 %collective-permute-start.3 = (bf16[2,128,512]{2,1,0:T(8,128)(2,1)S(1)}, bf16[2,128,512]{2,1,0:T(8,128)(2,1)S(1)}, u32[]{:S(2)}, u32[]{:S(2)}) collective-permute-start(bf16[2,128,512]{2,1,0:T(8,128)(2,1)S(1)} %shard_map.106), channel_id=1, source_target_pairs={{0,4},{2,6},{4,0},{6,2},{1,5},{3,7},{5,1},{7,3},{8,12},{10,14},{12... | collective-permute-start | bytes 786440 | tf_op jit(solution)/shard_map/ppermute | solution.py:192
  66.2 11.8 %collective-permute-start.2 = (bf16[2,128,512]{2,1,0:T(8,128)(2,1)S(1)}, bf16[2,128,512]{2,1,0:T(8,128)(2,1)S(1)}, u32[]{:S(2)}, u32[]{:S(2)}) collective-permute-start(bf16[2,128,512]{2,1,0:T(8,128)(2,1)S(1)} %shard_map.106), channel_id=1, source_target_pairs={{0,2},{2,4},{4,6},{6,0},{1,3},{3,5},{5,7},{7,1},{8,10},{10,12},{12... | collective-permute-start | bytes 786440 | tf_op jit(solution)/shard_map/ppermute | solution.py:192
  78.0 2.1 %copy-start.1 = (bf16[256,128]{1,0:T(8,128)(2,1)S(1)}, bf16[256,128]{1,0:T(8,128)(2,1)}, u32[]{:S(2)}) copy-start(bf16[256,128]{1,0:T(8,128)(2,1)} %keys_ref.3) | copy-start | bytes 196612
  78.0 2.1 %copy-start.2 = (bf16[256,128]{1,0:T(8,128)(2,1)S(1)}, bf16[256,128]{1,0:T(8,128)(2,1)}, u32[]{:S(2)}) copy-start(bf16[256,128]{1,0:T(8,128)(2,1)} %values_ref.3) | copy-start | bytes 196612
  78.0 2.1 %copy-start.3 = (bf16[256,128]{1,0:T(8,128)(2,1)S(1)}, bf16[256,128]{1,0:T(8,128)(2,1)}, u32[]{:S(2)}) copy-start(bf16[256,128]{1,0:T(8,128)(2,1)} %queries_ref.1) | copy-start | bytes 196612
  78.0 2.1 %copy-start.4 = (bf16[256,128]{1,0:T(8,128)(2,1)S(1)}, bf16[256,128]{1,0:T(8,128)(2,1)}, u32[]{:S(2)}) copy-start(bf16[256,128]{1,0:T(8,128)(2,1)} %grad_ref.1) | copy-start | bytes 196612
  78.0 2.1 %copy-start.5 = (f32[2,256]{1,0:T(2,128)S(1)}, f32[2,256]{1,0:T(2,128)}, u32[]{:S(2)}) copy-start(f32[2,256]{1,0:T(2,128)} %sums_ref.1) | copy-start | bytes 6148
  78.2 25.7 %collective-permute-start.5 = (bf16[4,2,128,512]{3,2,1,0:T(8,128)(2,1)S(1)}, bf16[4,2,128,512]{3,2,1,0:T(8,128)(2,1)S(1)}, u32[]{:S(2)}, u32[]{:S(2)}) collective-permute-start(bf16[4,2,128,512]{3,2,1,0:T(8,128)(2,1)S(1)} %pad_maximum_fusion.mine_ref), channel_id=1, source_target_pairs={{0,1},{1,0},{2,3},{3,2},{4,5},{5,4},{6,7},{7,6},{8,9},{9,8},{10,11... | collective-permute-start | bytes 3145736 | tf_op jit(solution)/shard_map/ppermute | solution.py:192
  82.5 37.5 %all-to-all-start.2 = ((bf16[64,16,128]{2,1,0:T(8,128)(2,1)}), bf16[64,16,128]{2,1,0:T(8,128)(2,1)S(1)}, u32[]{:S(2)}, u32[]{:S(2)}) async-start(bf16[64,16,128]{2,1,0:T(8,128)(2,1)} %bitcast.9), calls=%async_computation.2 | async-start | bytes 524288 | tf_op jit(solution)/shard_map/all_to_all | solution.py:187
  97.6 6.2 %collective-permute-start = (bf16[256,128]{1,0:T(8,128)(2,1)S(1)}, bf16[256,128]{1,0:T(8,128)(2,1)S(1)}, u32[]{:S(2)}, u32[]{:S(2)}) collective-permute-start(bf16[256,128]{1,0:T(8,128)(2,1)S(1)} %slice_bitcast_fusion), channel_id=1, source_target_pairs={{0,8},{8,0},{16,24},{24,16},{1,9},{9,1},{17,25},{25,17},{2,10},{10... | collective-permute-start | bytes 196616 | tf_op jit(solution)/shard_map/ppermute | solution.py:196

commit v4 on v3

--- a/solution.py
+++ b/solution.py
@@ -38,16 +38,14 @@
             here = lane == base_ref[0] + (g * SEL + s)
             high = jnp.where(here, (entry >> 3).astype(F32), high)
             low = jnp.where(here, (entry & 7).astype(F32), low)
-    row, col = iota((64 * 18, 512), 0), iota((64 * 18, 512), 1)
+    row = iota((64 * 18, 128), 0)
     piece = (row * 3641) >> 16
     kind = row - piece * 18
     source = jnp.where(kind < 8, kind * KB, 256 + (kind - 10) * KB) + (piece >> 1)
-    perm = one_hot(((kind < 8) | (kind >= 10)) & (col == source))
+    source = jnp.where((kind == 8) | (kind == 9), -1, source) - iota((64 * 18, 128), 1)
+    perm = jnp.concatenate([one_hot(source == n * 128) for n in range(4)], axis=1)
     pairs = jnp.concatenate([keys_ref[...], values_ref[...]], axis=1)
     both = dot(perm, jnp.concatenate([pairs, normed_ref[...]], axis=0))
-    row = iota((64 * 18, 128), 0)
-    piece = (row * 3641) >> 16
-    kind = row - piece * 18
     extra = jnp.where(kind == 8, high, 0.0) + jnp.where(kind == 9, low, 0.0)
     out_ref[...] = (jnp.where((piece & 1) == 0, both[:, :128], both[:, 128:]) + extra).astype(BF16)
 
@@ -62,9 +60,8 @@
     ids_ref[...] = ids
     columns = ids.T
     number = (iota((128, 512), 1) + 1).astype(F32)
-    for j in range(8):
-        hot = one_hot(number == columns[:, j : j + 1])
-        out_ref[j * 128 : (j + 1) * 128, :] = dot(hot, got).astype(BF16)
+    hot = jnp.concatenate([one_hot(number == columns[:, j : j + 1]) for j in range(8)], axis=0)
+    out_ref[...] = dot(hot, got).astype(BF16)
 
 
 def sent_kernel(y_ref, ids_ref, mine_ref, normed_ref, out_ref):
@@ -127,19 +124,17 @@
 
 def sum_kernel(y_ref, x_ref, c_ref, ids_ref, got_ref, own_ref, partner_ref, mine_ref, other_ref, out_ref):
     number = (iota((512, 128), 0) + 1).astype(F32)
-    sums = jnp.zeros((512, 128), F32)
-    for j in range(8):
-        hot = one_hot(number == ids_ref[j : j + 1, :])
-        sums = sums + dot(hot, got_ref[j * 128 : (j + 1) * 128, :])
+    hot = jnp.concatenate([one_hot(number == ids_ref[j : j + 1, :]) for j in range(8)], axis=1)
+    sums = dot(hot, got_ref[...])
     owned = jnp.concatenate([own_ref[1], partner_ref[...]], axis=0).astype(F32)
     value = jnp.where((y_ref[0] & 1) == 1, sums, owned).astype(BF16)
     for c, features_ref in enumerate((mine_ref, other_ref)):
+        part = dot(features_ref[...].reshape(1024, 512), value).astype(BF16).reshape(4, 2, 4, 32, 128)
         for s in range(4):
             t = ((x_ref[0] - s) & 3) * 2 + ((c_ref[0] + c) & 1)
-            part = dot(features_ref[s].reshape(256, 512), value).astype(BF16).reshape(2, 4, 32, 128)
             for zz in range(2):
                 for y in range(4):
-                    out_ref[y, t * 2 + zz] = part[zz, y]
+                    out_ref[y, t * 2 + zz] = part[s, zz, y]
     sums = sums.reshape(4, 4, 4, 8, 128)
     for y in range(4):
         out_ref[y, 16:] = sums[:, :, y].reshape(4, 32, 128).astype(BF16)
@@ -157,10 +152,11 @@
 def last_kernel(got_ref, own_ref, dk_ref, dv_ref, total_ref):
     total_ref[...] = got_ref[:, :32].astype(F32).sum(axis=0)
     sums = got_ref[:, 32:].reshape(512, 128)
-    row, col = iota((256, 512), 0), iota((256, 512), 1)
-    first = (row & 31) * 16 + (row >> 5)
-    dk_ref[...] = (dot(one_hot(col == first), sums) + own_ref[0].astype(F32)).astype(BF16)
-    dv_ref[...] = (dot(one_hot(col == first + 8), sums) + own_ref[1].astype(F32)).astype(BF16)
+    row = iota((256, 128), 0)
+    first = (row & 31) * 16 + (row >> 5) - iota((256, 128), 1)
+    for n, ref in enumerate((dk_ref, dv_ref)):
+        perm = jnp.concatenate([one_hot(first == m * 128 - n * 8) for m in range(4)], axis=1)
+        ref[...] = (dot(perm, sums) + own_ref[n].astype(F32)).astype(BF16)
 
 
 VM = pl.BlockSpec(memory_space=pltpu.VMEM)
@@ -224,7 +220,7 @@
         hbm=(0,),
     )
     back = exchange(back.reshape(64, 16, 128), KV)
-    partner = swapped(own[1])
+    partner = lax.ppermute(own[1], "y", [(1, 0), (3, 2)])
     (sums,) = call(
         sum_kernel,
         [shape(4, 20, 32, 128)],

time: 158 us -> 158 us (level)
  starting transfers between devices: 39.7 us -> 37.6 us
  waiting for transfers between devices: 31.9 us -> 33.9 us
    ppermute x0 -> x1, waiting for transfers between devices: none -> 4.94 us  [body(): partner = lax.ppermute(own[1], 'y', [(1, 0), (3, 2)])]
    ppermute x2 -> x1, starting transfers between devices: 6.74 us -> 3.37 us  [swapped(): return lax.ppermute(x, 'y', [(n, n ^ 1) for n in range(4)])]
    ppermute x2 -> x1, waiting for transfers between devices: 6.65 us -> 3.79 us  [swapped(): return lax.ppermute(x, 'y', [(n, n ^ 1) for n in range(4)])]
where the time goes in v4:
time: 158 us; the launch traced here: 157 us
  blocking collectives  76.1 us (48%)
  starting transfers between devices  37.6 us (24%)
  waiting for transfers between devices  33.9 us (21%)
  Pallas kernels  8.45 us (5%)
    all_to_all x3, blocking collectives, exchange(): return lax.all_to_all(x, axis, split_axis=0, concat_axis=0, tiled=True)  76.1 us
    all_to_all x2, starting transfers between devices, exchange(): return lax.all_to_all(x, axis, split_axis=0, concat_axis=0, tiled=True)  20.9 us
    all_to_all x2, waiting for transfers between devices, exchange(): return lax.all_to_all(x, axis, split_axis=0, concat_axis=0, tiled=True)  16.2 us
    ppermute x4, starting transfers between devices, shift(): return lax.ppermute(x, axis, [(n, (n + by) % size) for n in range(size)])  12.1 us
    ppermute x4, waiting for transfers between devices, shift(): return lax.ppermute(x, axis, [(n, (n + by) % size) for n in range(size)])  8.98 us
    pallas_call x8, Pallas kernels, call(): pl.pallas_call(kernel, out_shape=[o if n in hbm else pltpu.VMEM(o.shape,...  8.45 us
    ppermute x1, waiting for transfers between devices, body(): partner = lax.ppermute(own[1], 'y', [(1, 0), (3, 2)])  4.94 us
    ppermute x1, waiting for transfers between devices, swapped(): return lax.ppermute(x, 'y', [(n, n ^ 1) for n in range(4)])  3.79 us
  transfers between devices with their start and end apart: 8, of which 6 were waited for; matrix products, arithmetic and copies ran while one was open for 0% of the time, Pallas kernels for 2%

profile of v4, /device:TPU:32, one launch (start us, length us, event | category | flops | bytes accessed | tf_op | source)
XLA Modules:
  0.0 157.3 jit_solution(3889361968214286253)
XLA Ops:
  0.6 1.7 %shard_map.102 = bf16[1152,128]{1,0:T(8,128)(2,1)S(1)} custom-call(s32[1]{0:T(128)} %bitcast.base_ref, s32[2,8]{1,0:T(2,128)} %chosen_ref.3, bf16[256,128]{1,0:T(8,128)(2,1)} %keys_ref.3, bf16[256,128]{1,0:T(8,128)(2,1)} %values_ref.3, bf16[256,256]{1,0:T(8,128)(2,1)} %normed_ref.5), custom_call_target="tpu_custom_call" | custom-call | tf_op jit(solution)/shard_map/pallas_call | solution.py:169
  2.3 41.3 %all_to_all.25 = bf16[64,9,2,128]{3,2,1,0:T(2,128)(2,1)S(1)} all-to-all(bf16[64,9,2,128]{3,2,1,0:T(2,128)(2,1)S(1)} %bitcast.18), channel_id=1, replica_groups=mesh['z'=16,'y'=4,'x'=4,'c'=2] {'z','y'}, dimensions={0} | all-to-all | bytes 589824 | tf_op jit(solution)/shard_map/all_to_all | solution.py:183
  43.7 0.2 fusion
  43.9 1.4 shard_map.103
  45.3 0.0 copy-start
  45.3 5.8 %all-to-all-start.1 = ((bf16[64,16,128]{2,1,0:T(8,128)(2,1)}), bf16[64,16,128]{2,1,0:T(8,128)(2,1)S(1)}, u32[]{:S(2)}, u32[]{:S(2)}) async-start(bf16[64,16,128]{2,1,0:T(8,128)(2,1)} %bitcast.4), calls=%async_computation.1 | async-start | bytes 524288 | tf_op jit(solution)/shard_map/all_to_all | solution.py:183
  51.1 0.0 copy-done
  51.1 3.4 %collective-permute-start.1 = (bf16[512,128]{1,0:T(8,128)(2,1)S(1)}, bf16[512,128]{1,0:T(8,128)(2,1)S(1)}, u32[]{:S(2)}, u32[]{:S(2)}) collective-permute-start(bf16[512,128]{1,0:T(8,128)(2,1)S(1)} %shard_map.105), channel_id=1, source_target_pairs={{0,8},{8,0},{16,24},{24,16},{1,9},{9,1},{17,25},{25,17},{2,10},{10... | collective-permute-start | bytes 393224 | tf_op jit(solution)/shard_map/ppermute | solution.py:192
  54.5 3.8 %collective-permute-done.1.other_ref = bf16[512,128]{1,0:T(8,128)(2,1)S(1)} collective-permute-done((bf16[512,128]{1,0:T(8,128)(2,1)S(1)}, bf16[512,128]{1,0:T(8,128)(2,1)S(1)}, u32[]{:S(2)}, u32[]{:S(2)}) %collective-permute-start.1) | collective-permute-done | bytes 131104 | tf_op jit(solution)/shard_map/ppermute | solution.py:192
  58.3 0.4 shard_map.106
  58.7 4.7 %collective-permute-start.4 = (bf16[2,128,512]{2,1,0:T(8,128)(2,1)S(1)}, bf16[2,128,512]{2,1,0:T(8,128)(2,1)S(1)}, u32[]{:S(2)}, u32[]{:S(2)}) collective-permute-start(bf16[2,128,512]{2,1,0:T(8,128)(2,1)S(1)} %shard_map.106), channel_id=1, source_target_pairs={{0,6},{2,0},{4,2},{6,4},{1,7},{3,1},{5,3},{7,5},{8,14},{10,8},{12,... | collective-permute-start | bytes 786440 | tf_op jit(solution)/shard_map/ppermute | solution.py:188
  63.4 2.7 %collective-permute-start.3 = (bf16[2,128,512]{2,1,0:T(8,128)(2,1)S(1)}, bf16[2,128,512]{2,1,0:T(8,128)(2,1)S(1)}, u32[]{:S(2)}, u32[]{:S(2)}) collective-permute-start(bf16[2,128,512]{2,1,0:T(8,128)(2,1)S(1)} %shard_map.106), channel_id=1, source_target_pairs={{0,4},{2,6},{4,0},{6,2},{1,5},{3,7},{5,1},{7,3},{8,12},{10,14},{12... | collective-permute-start | bytes 786440 | tf_op jit(solution)/shard_map/ppermute | solution.py:188
  66.1 2.8 %collective-permute-start.2 = (bf16[2,128,512]{2,1,0:T(8,128)(2,1)S(1)}, bf16[2,128,512]{2,1,0:T(8,128)(2,1)S(1)}, u32[]{:S(2)}, u32[]{:S(2)}) collective-permute-start(bf16[2,128,512]{2,1,0:T(8,128)(2,1)S(1)} %shard_map.106), channel_id=1, source_target_pairs={{0,2},{2,4},{4,6},{6,0},{1,3},{3,5},{5,7},{7,1},{8,10},{10,12},{12... | collective-permute-start | bytes 786440 | tf_op jit(solution)/shard_map/ppermute | solution.py:188
  68.9 3.7 %collective-permute-done.4 = bf16[2,128,512]{2,1,0:T(8,128)(2,1)S(1)} collective-permute-done((bf16[2,128,512]{2,1,0:T(8,128)(2,1)S(1)}, bf16[2,128,512]{2,1,0:T(8,128)(2,1)S(1)}, u32[]{:S(2)}, u32[]{:S(2)}) %collective-permute-start.4) | collective-permute-done | bytes 262176 | tf_op jit(solution)/shard_map/ppermute | solution.py:188
  72.6 2.5 %collective-permute-done.3 = bf16[2,128,512]{2,1,0:T(8,128)(2,1)S(1)} collective-permute-done((bf16[2,128,512]{2,1,0:T(8,128)(2,1)S(1)}, bf16[2,128,512]{2,1,0:T(8,128)(2,1)S(1)}, u32[]{:S(2)}, u32[]{:S(2)}) %collective-permute-start.3) | collective-permute-done | bytes 262176 | tf_op jit(solution)/shard_map/ppermute | solution.py:188
  75.1 2.8 %collective-permute-done.2 = bf16[2,128,512]{2,1,0:T(8,128)(2,1)S(1)} collective-permute-done((bf16[2,128,512]{2,1,0:T(8,128)(2,1)S(1)}, bf16[2,128,512]{2,1,0:T(8,128)(2,1)S(1)}, u32[]{:S(2)}, u32[]{:S(2)}) %collective-permute-start.2) | collective-permute-done | bytes 262176 | tf_op jit(solution)/shard_map/ppermute | solution.py:188
  77.9 0.0 copy-start.1
  77.9 0.0 copy-start.2
  77.9 0.0 copy-start.3
  77.9 0.0 copy-start.4
  77.9 0.0 copy-start.5
  77.9 0.1 pad_maximum_fusion.mine_ref
  78.0 1.9 %collective-permute-start.5 = (bf16[4,2,128,512]{3,2,1,0:T(8,128)(2,1)S(1)}, bf16[4,2,128,512]{3,2,1,0:T(8,128)(2,1)S(1)}, u32[]{:S(2)}, u32[]{:S(2)}) collective-permute-start(bf16[4,2,128,512]{3,2,1,0:T(8,128)(2,1)S(1)} %pad_maximum_fusion.mine_ref), channel_id=1, source_target_pairs={{0,1},{1,0},{2,3},{3,2},{4,5},{5,4},{6,7},{7,6},{8,9},{9,8},{10,11... | collective-permute-start | bytes 3145736 | tf_op jit(solution)/shard_map/ppermute | solution.py:188
  80.0 0.0 all-to-all-done.1
  80.0 0.0 copy-done.1
  80.0 0.0 copy-done.2
  80.0 0.0 copy-done.3
  80.0 0.0 copy-done.4
  80.0 0.0 copy-done.5
  80.0 2.4 %shard_map.104 = (bf16[256,128]{1,0:T(8,128)(2,1)}, bf16[32,2,16,128]{3,2,1,0:T(8,128)(2,1)}, bf16[2,256,128]{2,1,0:T(8,128)(2,1)S(1)}) custom-call(s32[2,8]{1,0:T(2,128)} %chosen_ref.3, bf16[256,128]{1,0:T(8,128)(2,1)S(1)} %copy-done.3, bf16[256,128]{1,0:T(8,128)(2,1)S(1)} %copy-done.1, bf16[256,128]{1,0:T(8,128)(2,1)S(1)} %copy-done.2, ...), custom_call_target="tpu_custom_call" | custom-call | tf_op jit(solution)/shard_map/pallas_call | solution.py:169
  82.4 15.1 %all-to-all-start.2 = ((bf16[64,16,128]{2,1,0:T(8,128)(2,1)}), bf16[64,16,128]{2,1,0:T(8,128)(2,1)S(1)}, u32[]{:S(2)}, u32[]{:S(2)}) async-start(bf16[64,16,128]{2,1,0:T(8,128)(2,1)} %bitcast.9), calls=%async_computation.2 | async-start | bytes 524288 | tf_op jit(solution)/shard_map/all_to_all | solution.py:183
  97.5 1.3 collective-permute-start
  98.8 4.9 %collective-permute-done.partner_ref = bf16[256,128]{1,0:T(8,128)(2,1)S(1)} collective-permute-done((bf16[256,128]{1,0:T(8,128)(2,1)S(1)}, bf16[256,128]{1,0:T(8,128)(2,1)S(1)}, u32[]{:S(2)}, u32[]{:S(2)}) %collective-permute-start) | collective-permute-done | bytes 65568 | tf_op jit(solution)/shard_map/ppermute | solution.py:223
  103.8 0.0 collective-permute-done.5.other_ref
  103.8 16.2 %all-to-all-done.2 = bf16[64,16,128]{2,1,0:T(8,128)(2,1)S(1)} async-done(((bf16[64,16,128]{2,1,0:T(8,128)(2,1)}), bf16[64,16,128]{2,1,0:T(8,128)(2,1)S(1)}, u32[]{:S(2)}, u32[]{:S(2)}) %all-to-all-start.2) | async-done | bytes 262176 | tf_op jit(solution)/shard_map/all_to_all | solution.py:183
  120.0 1.5 shard_map.107
  121.5 12.0 %all_to_all.26.got_ref = bf16[4,20,32,128]{3,2,1,0:T(8,128)(2,1)S(1)} all-to-all(bf16[4,20,32,128]{3,2,1,0:T(8,128)(2,1)S(1)} %shard_map.107), channel_id=1, replica_groups=mesh['z'=16,'y'=4,'x'=4,'c'=2] {'y'}, dimensions={0} | all-to-all | bytes 1310720 | tf_op jit(solution)/shard_map/all_to_all | solution.py:183
  133.6 0.1 shard_map.108
  133.6 22.7 %all_to_all.27.got_ref = bf16[16,64,128]{2,1,0:T(8,128)(2,1)S(1)} all-to-all(bf16[16,64,128]{2,1,0:T(8,128)(2,1)S(1)} %shard_map.108), channel_id=1, replica_groups=mesh['z'=16,'y'=4,'x'=4,'c'=2] {'z'}, dimensions={0} | all-to-all | bytes 524288 | tf_op jit(solution)/shard_map/all_to_all | solution.py:183
  156.4 0.9 shard_map.109
  (3 shorter events, 0.1 us)
Async XLA Ops:
  45.3 5.8 %copy-start = (bf16[256,256]{1,0:T(8,128)(2,1)S(1)}, bf16[256,256]{1,0:T(8,128)(2,1)}, u32[]{:S(2)}) copy-start(bf16[256,256]{1,0:T(8,128)(2,1)} %normed_ref.5) | copy-start | bytes 393220
  45.3 34.7 %all-to-all-start.1 = ((bf16[64,16,128]{2,1,0:T(8,128)(2,1)}), bf16[64,16,128]{2,1,0:T(8,128)(2,1)S(1)}, u32[]{:S(2)}, u32[]{:S(2)}) async-start(bf16[64,16,128]{2,1,0:T(8,128)(2,1)} %bitcast.4), calls=%async_computation.1 | async-start | bytes 524288 | tf_op jit(solution)/shard_map/all_to_all | solution.py:183
  51.1 7.2 %collective-permute-start.1 = (bf16[512,128]{1,0:T(8,128)(2,1)S(1)}, bf16[512,128]{1,0:T(8,128)(2,1)S(1)}, u32[]{:S(2)}, u32[]{:S(2)}) collective-permute-start(bf16[512,128]{1,0:T(8,128)(2,1)S(1)} %shard_map.105), channel_id=1, source_target_pairs={{0,8},{8,0},{16,24},{24,16},{1,9},{9,1},{17,25},{25,17},{2,10},{10... | collective-permute-start | bytes 393224 | tf_op jit(solution)/shard_map/ppermute | solution.py:192
  58.7 13.9 %collective-permute-start.4 = (bf16[2,128,512]{2,1,0:T(8,128)(2,1)S(1)}, bf16[2,128,512]{2,1,0:T(8,128)(2,1)S(1)}, u32[]{:S(2)}, u32[]{:S(2)}) collective-permute-start(bf16[2,128,512]{2,1,0:T(8,128)(2,1)S(1)} %shard_map.106), channel_id=1, source_target_pairs={{0,6},{2,0},{4,2},{6,4},{1,7},{3,1},{5,3},{7,5},{8,14},{10,8},{12,... | collective-permute-start | bytes 786440 | tf_op jit(solution)/shard_map/ppermute | solution.py:188
  63.4 11.7 %collective-permute-start.3 = (bf16[2,128,512]{2,1,0:T(8,128)(2,1)S(1)}, bf16[2,128,512]{2,1,0:T(8,128)(2,1)S(1)}, u32[]{:S(2)}, u32[]{:S(2)}) collective-permute-start(bf16[2,128,512]{2,1,0:T(8,128)(2,1)S(1)} %shard_map.106), channel_id=1, source_target_pairs={{0,4},{2,6},{4,0},{6,2},{1,5},{3,7},{5,1},{7,3},{8,12},{10,14},{12... | collective-permute-start | bytes 786440 | tf_op jit(solution)/shard_map/ppermute | solution.py:188
  66.1 11.8 %collective-permute-start.2 = (bf16[2,128,512]{2,1,0:T(8,128)(2,1)S(1)}, bf16[2,128,512]{2,1,0:T(8,128)(2,1)S(1)}, u32[]{:S(2)}, u32[]{:S(2)}) collective-permute-start(bf16[2,128,512]{2,1,0:T(8,128)(2,1)S(1)} %shard_map.106), channel_id=1, source_target_pairs={{0,2},{2,4},{4,6},{6,0},{1,3},{3,5},{5,7},{7,1},{8,10},{10,12},{12... | collective-permute-start | bytes 786440 | tf_op jit(solution)/shard_map/ppermute | solution.py:188
  77.9 2.1 %copy-start.1 = (bf16[256,128]{1,0:T(8,128)(2,1)S(1)}, bf16[256,128]{1,0:T(8,128)(2,1)}, u32[]{:S(2)}) copy-start(bf16[256,128]{1,0:T(8,128)(2,1)} %keys_ref.3) | copy-start | bytes 196612
  77.9 2.1 %copy-start.2 = (bf16[256,128]{1,0:T(8,128)(2,1)S(1)}, bf16[256,128]{1,0:T(8,128)(2,1)}, u32[]{:S(2)}) copy-start(bf16[256,128]{1,0:T(8,128)(2,1)} %values_ref.3) | copy-start | bytes 196612
  77.9 2.1 %copy-start.3 = (bf16[256,128]{1,0:T(8,128)(2,1)S(1)}, bf16[256,128]{1,0:T(8,128)(2,1)}, u32[]{:S(2)}) copy-start(bf16[256,128]{1,0:T(8,128)(2,1)} %queries_ref.1) | copy-start | bytes 196612
  77.9 2.1 %copy-start.4 = (bf16[256,128]{1,0:T(8,128)(2,1)S(1)}, bf16[256,128]{1,0:T(8,128)(2,1)}, u32[]{:S(2)}) copy-start(bf16[256,128]{1,0:T(8,128)(2,1)} %grad_ref.1) | copy-start | bytes 196612
  77.9 2.1 %copy-start.5 = (f32[2,256]{1,0:T(2,128)S(1)}, f32[2,256]{1,0:T(2,128)}, u32[]{:S(2)}) copy-start(f32[2,256]{1,0:T(2,128)} %sums_ref.1) | copy-start | bytes 6148
  78.0 25.7 %collective-permute-start.5 = (bf16[4,2,128,512]{3,2,1,0:T(8,128)(2,1)S(1)}, bf16[4,2,128,512]{3,2,1,0:T(8,128)(2,1)S(1)}, u32[]{:S(2)}, u32[]{:S(2)}) collective-permute-start(bf16[4,2,128,512]{3,2,1,0:T(8,128)(2,1)S(1)} %pad_maximum_fusion.mine_ref), channel_id=1, source_target_pairs={{0,1},{1,0},{2,3},{3,2},{4,5},{5,4},{6,7},{7,6},{8,9},{9,8},{10,11... | collective-permute-start | bytes 3145736 | tf_op jit(solution)/shard_map/ppermute | solution.py:188
  82.4 37.5 %all-to-all-start.2 = ((bf16[64,16,128]{2,1,0:T(8,128)(2,1)}), bf16[64,16,128]{2,1,0:T(8,128)(2,1)S(1)}, u32[]{:S(2)}, u32[]{:S(2)}) async-start(bf16[64,16,128]{2,1,0:T(8,128)(2,1)} %bitcast.9), calls=%async_computation.2 | async-start | bytes 524288 | tf_op jit(solution)/shard_map/all_to_all | solution.py:183
  97.5 6.2 %collective-permute-start = (bf16[256,128]{1,0:T(8,128)(2,1)S(1)}, bf16[256,128]{1,0:T(8,128)(2,1)S(1)}, u32[]{:S(2)}, u32[]{:S(2)}) collective-permute-start(bf16[256,128]{1,0:T(8,128)(2,1)S(1)} %slice_bitcast_fusion), channel_id=1, source_target_pairs={{8,0},{24,16},{9,1},{25,17},{10,2},{26,18},{11,3},{27,19},{12,4},{... | collective-permute-start | bytes 196616 | tf_op jit(solution)/shard_map/ppermute | solution.py:223

commit v5 on v4

--- a/solution.py
+++ b/solution.py
@@ -82,12 +82,11 @@
 
 
 def attend_kernel(
-    chosen_ref, queries_ref, keys_ref, values_ref, grad_ref, sums_ref, got_ref, dq_ref, back_ref, own_ref
+    chosen_ref, queries_ref, keys_ref, values_ref, grad_ref, sums_ref, got_ref, back_ref, slopes_ref, low_ref
 ):
     mine = (iota((2 * QB, 128), 1) >= HD) == (iota((2 * QB, 128), 0) >= QB)
     causal = iota((QB, 2 * QB), 0) <= (iota((QB, 2 * QB), 1) & (QB - 1))
     sub = iota((SEL, 2 * QB), 0)
-    low_lanes = iota((QB, 128), 1) < HD
     for g in range(2):
         span = slice(g * QB, (g + 1) * QB)
         picked = []
@@ -112,13 +111,29 @@
         low = weights.astype(BF16)
         deltas = jnp.sum(low.astype(F32) * dots, axis=0, keepdims=True)
         slopes = (weights * (dots - deltas)).astype(BF16)
-        dk = dot(slopes, q)
-        dv = dot(low, do)
+        slopes_ref[g] = slopes
+        low_ref[g] = low
+        dk = dot(slopes[: KB * SEL], q)
+        dv = dot(low[: KB * SEL], do)
+        back_ref[:, 0, g * SEL : (g + 1) * SEL, :] = dk.reshape(KB, SEL, 128).astype(BF16)
+        back_ref[:, 1, g * SEL : (g + 1) * SEL, :] = dv.reshape(KB, SEL, 128).astype(BF16)
+
+
+def rest_kernel(queries_ref, keys_ref, grad_ref, got_ref, slopes_ref, low_ref, dq_ref, own_ref):
+    mine = (iota((2 * QB, 128), 1) >= HD) == (iota((2 * QB, 128), 0) >= QB)
+    low_lanes = iota((QB, 128), 1) < HD
+    for g in range(2):
+        span = slice(g * QB, (g + 1) * QB)
+        picked = got_ref[:, 0, g * SEL : (g + 1) * SEL, :].reshape(KB * SEL, 128)
+        keys = jnp.concatenate([picked, keys_ref[span, :]], axis=0)
+        q = queries_ref[span, :].astype(F32) * (HD**-0.5)
+        do = grad_ref[span, :].astype(F32)
+        q = jnp.where(mine, jnp.concatenate([q, q], axis=0), 0.0).astype(BF16)
+        do = jnp.where(mine, jnp.concatenate([do, do], axis=0), 0.0).astype(BF16)
+        slopes = slopes_ref[g]
+        own_ref[0, span, :] = dot(slopes[KB * SEL :], q).astype(BF16)
+        own_ref[1, span, :] = dot(low_ref[g, KB * SEL :, :], do).astype(BF16)
         dq = dot(slopes, keys, ((0,), (0,)))
-        back_ref[:, 0, g * SEL : (g + 1) * SEL, :] = dk[: KB * SEL].reshape(KB, SEL, 128).astype(BF16)
-        back_ref[:, 1, g * SEL : (g + 1) * SEL, :] = dv[: KB * SEL].reshape(KB, SEL, 128).astype(BF16)
-        own_ref[0, span, :] = dk[KB * SEL :].astype(BF16)
-        own_ref[1, span, :] = dv[KB * SEL :].astype(BF16)
         dq_ref[span, :] = (jnp.where(low_lanes, dq[:QB], dq[QB:]) * (HD**-0.5)).astype(BF16)
 
 
@@ -212,11 +227,18 @@
         parts.append(shift(features, "x", s))
     features = jnp.stack(parts)
     others = shift(features, "c", 1)
-    query_grad, back, own = call(
+    picked = picked.reshape(KB, 2, 16, 128)
+    back, slopes, low = call(
         attend_kernel,
-        [shape(rows, 128), shape(KB, 2, 16, 128), shape(2, rows, 128)],
+        [shape(KB, 2, 16, 128), shape(2, 384, 256), shape(2, 384, 256)],
         [SM] + [VM] * 6,
-        chosen, queries, keys, values, out_grad, log_sums, picked.reshape(KB, 2, 16, 128),
+        chosen, queries, keys, values, out_grad, log_sums, picked,
+    )
+    query_grad, own = call(
+        rest_kernel,
+        [shape(rows, 128), shape(2, rows, 128)],
+        [VM] * 6,
+        queries, keys, out_grad, picked, slopes, low,
         hbm=(0,),
     )
     back = exchange(back.reshape(64, 16, 128), KV)

time: 158 us -> 159 us (level)
  Pallas kernels: 8.45 us -> 10.6 us
    pallas_call x8 -> x9, Pallas kernels: 8.45 us -> 10.6 us  [call(): pl.pallas_call(kernel, out_shape=[o if n in hbm else pltpu.VMEM(o.shape,...]
where the time goes in v5:
time: 159 us; the launch traced here: 158 us
  blocking collectives  76.1 us (48%)
  starting transfers between devices  37.6 us (24%)
  waiting for transfers between devices  33 us (21%)
  Pallas kernels  10.6 us (7%)
    all_to_all x3, blocking collectives, exchange(): return lax.all_to_all(x, axis, split_axis=0, concat_axis=0, tiled=True)  76.1 us
    all_to_all x2, starting transfers between devices, exchange(): return lax.all_to_all(x, axis, split_axis=0, concat_axis=0, tiled=True)  20.9 us
    all_to_all x2, waiting for transfers between devices, exchange(): return lax.all_to_all(x, axis, split_axis=0, concat_axis=0, tiled=True)  15.2 us
    ppermute x4, starting transfers between devices, shift(): return lax.ppermute(x, axis, [(n, (n + by) % size) for n in range(size)])  12.1 us
    pallas_call x9, Pallas kernels, call(): pl.pallas_call(kernel, out_shape=[o if n in hbm else pltpu.VMEM(o.shape,...  10.6 us
    ppermute x4, waiting for transfers between devices, shift(): return lax.ppermute(x, axis, [(n, (n + by) % size) for n in range(size)])  8.99 us
    ppermute x1, waiting for transfers between devices, body(): partner = lax.ppermute(own[1], 'y', [(1, 0), (3, 2)])  5.03 us
    ppermute x1, waiting for transfers between devices, swapped(): return lax.ppermute(x, 'y', [(n, n ^ 1) for n in range(4)])  3.79 us
  transfers between devices with their start and end apart: 8, of which 6 were waited for; matrix products, arithmetic and copies ran while one was open for 0% of the time, Pallas kernels for 2%

profile of v5, /device:TPU:32, one launch (start us, length us, event | category | flops | bytes accessed | tf_op | source)
XLA Modules:
  0.0 158.5 jit_solution(8980509481728828177)
XLA Ops:
  0.6 1.7 %shard_map.102 = bf16[1152,128]{1,0:T(8,128)(2,1)S(1)} custom-call(s32[1]{0:T(128)} %bitcast.base_ref, s32[2,8]{1,0:T(2,128)} %chosen_ref.3, bf16[256,128]{1,0:T(8,128)(2,1)} %keys_ref.5, bf16[256,128]{1,0:T(8,128)(2,1)} %values_ref.3, bf16[256,256]{1,0:T(8,128)(2,1)} %normed_ref.5), custom_call_target="tpu_custom_call" | custom-call | tf_op jit(solution)/shard_map/pallas_call | solution.py:184
  2.3 41.3 %all_to_all.25 = bf16[64,9,2,128]{3,2,1,0:T(2,128)(2,1)S(1)} all-to-all(bf16[64,9,2,128]{3,2,1,0:T(2,128)(2,1)S(1)} %bitcast.20), channel_id=1, replica_groups=mesh['z'=16,'y'=4,'x'=4,'c'=2] {'z','y'}, dimensions={0} | all-to-all | bytes 589824 | tf_op jit(solution)/shard_map/all_to_all | solution.py:198
  43.7 0.2 fusion
  43.9 1.4 shard_map.103
  45.3 0.0 copy-start
  45.3 5.8 %all-to-all-start.1 = ((bf16[64,16,128]{2,1,0:T(8,128)(2,1)}), bf16[64,16,128]{2,1,0:T(8,128)(2,1)S(1)}, u32[]{:S(2)}, u32[]{:S(2)}) async-start(bf16[64,16,128]{2,1,0:T(8,128)(2,1)} %bitcast.4), calls=%async_computation.1 | async-start | bytes 524288 | tf_op jit(solution)/shard_map/all_to_all | solution.py:198
  51.1 0.0 copy-done
  51.2 3.4 %collective-permute-start.1 = (bf16[512,128]{1,0:T(8,128)(2,1)S(1)}, bf16[512,128]{1,0:T(8,128)(2,1)S(1)}, u32[]{:S(2)}, u32[]{:S(2)}) collective-permute-start(bf16[512,128]{1,0:T(8,128)(2,1)S(1)} %shard_map.106), channel_id=1, source_target_pairs={{0,8},{8,0},{16,24},{24,16},{1,9},{9,1},{17,25},{25,17},{2,10},{10... | collective-permute-start | bytes 393224 | tf_op jit(solution)/shard_map/ppermute | solution.py:207
  54.6 3.8 %collective-permute-done.1.other_ref = bf16[512,128]{1,0:T(8,128)(2,1)S(1)} collective-permute-done((bf16[512,128]{1,0:T(8,128)(2,1)S(1)}, bf16[512,128]{1,0:T(8,128)(2,1)S(1)}, u32[]{:S(2)}, u32[]{:S(2)}) %collective-permute-start.1) | collective-permute-done | bytes 131104 | tf_op jit(solution)/shard_map/ppermute | solution.py:207
  58.3 0.4 shard_map.107
  58.7 4.7 %collective-permute-start.4 = (bf16[2,128,512]{2,1,0:T(8,128)(2,1)S(1)}, bf16[2,128,512]{2,1,0:T(8,128)(2,1)S(1)}, u32[]{:S(2)}, u32[]{:S(2)}) collective-permute-start(bf16[2,128,512]{2,1,0:T(8,128)(2,1)S(1)} %shard_map.107), channel_id=1, source_target_pairs={{0,6},{2,0},{4,2},{6,4},{1,7},{3,1},{5,3},{7,5},{8,14},{10,8},{12,... | collective-permute-start | bytes 786440 | tf_op jit(solution)/shard_map/ppermute | solution.py:203
  63.4 2.7 %collective-permute-start.3 = (bf16[2,128,512]{2,1,0:T(8,128)(2,1)S(1)}, bf16[2,128,512]{2,1,0:T(8,128)(2,1)S(1)}, u32[]{:S(2)}, u32[]{:S(2)}) collective-permute-start(bf16[2,128,512]{2,1,0:T(8,128)(2,1)S(1)} %shard_map.107), channel_id=1, source_target_pairs={{0,4},{2,6},{4,0},{6,2},{1,5},{3,7},{5,1},{7,3},{8,12},{10,14},{12... | collective-permute-start | bytes 786440 | tf_op jit(solution)/shard_map/ppermute | solution.py:203
  66.1 2.8 %collective-permute-start.2 = (bf16[2,128,512]{2,1,0:T(8,128)(2,1)S(1)}, bf16[2,128,512]{2,1,0:T(8,128)(2,1)S(1)}, u32[]{:S(2)}, u32[]{:S(2)}) collective-permute-start(bf16[2,128,512]{2,1,0:T(8,128)(2,1)S(1)} %shard_map.107), channel_id=1, source_target_pairs={{0,2},{2,4},{4,6},{6,0},{1,3},{3,5},{5,7},{7,1},{8,10},{10,12},{12... | collective-permute-start | bytes 786440 | tf_op jit(solution)/shard_map/ppermute | solution.py:203
  68.9 3.7 %collective-permute-done.4 = bf16[2,128,512]{2,1,0:T(8,128)(2,1)S(1)} collective-permute-done((bf16[2,128,512]{2,1,0:T(8,128)(2,1)S(1)}, bf16[2,128,512]{2,1,0:T(8,128)(2,1)S(1)}, u32[]{:S(2)}, u32[]{:S(2)}) %collective-permute-start.4) | collective-permute-done | bytes 262176 | tf_op jit(solution)/shard_map/ppermute | solution.py:203
  72.6 2.5 %collective-permute-done.3 = bf16[2,128,512]{2,1,0:T(8,128)(2,1)S(1)} collective-permute-done((bf16[2,128,512]{2,1,0:T(8,128)(2,1)S(1)}, bf16[2,128,512]{2,1,0:T(8,128)(2,1)S(1)}, u32[]{:S(2)}, u32[]{:S(2)}) %collective-permute-start.3) | collective-permute-done | bytes 262176 | tf_op jit(solution)/shard_map/ppermute | solution.py:203
  75.1 2.8 %collective-permute-done.2 = bf16[2,128,512]{2,1,0:T(8,128)(2,1)S(1)} collective-permute-done((bf16[2,128,512]{2,1,0:T(8,128)(2,1)S(1)}, bf16[2,128,512]{2,1,0:T(8,128)(2,1)S(1)}, u32[]{:S(2)}, u32[]{:S(2)}) %collective-permute-start.2) | collective-permute-done | bytes 262176 | tf_op jit(solution)/shard_map/ppermute | solution.py:203
  77.9 0.0 copy-start.1
  77.9 0.0 copy-start.2
  77.9 0.0 copy-start.3
  77.9 0.0 copy-start.4
  77.9 0.0 copy-start.5
  77.9 0.1 pad_maximum_fusion.mine_ref
  78.1 1.9 %collective-permute-start.5 = (bf16[4,2,128,512]{3,2,1,0:T(8,128)(2,1)S(1)}, bf16[4,2,128,512]{3,2,1,0:T(8,128)(2,1)}, u32[]{:S(2)}, u32[]{:S(2)}) collective-permute-start(bf16[4,2,128,512]{3,2,1,0:T(8,128)(2,1)S(1)} %pad_maximum_fusion.mine_ref), channel_id=1, source_target_pairs={{0,1},{1,0},{2,3},{3,2},{4,5},{5,4},{6,7},{7,6},{8,9},{9,8},{10,11... | collective-permute-start | bytes 3145736 | tf_op jit(solution)/shard_map/ppermute | solution.py:203
  80.0 0.0 all-to-all-done.1
  80.0 0.0 copy-done.1
  80.0 0.0 copy-done.2
  80.0 0.0 copy-done.3
  80.0 0.0 copy-done.4
  80.1 0.0 copy-done.5
  80.1 2.3 %shard_map.104 = (bf16[32,2,16,128]{3,2,1,0:T(8,128)(2,1)}, bf16[2,384,256]{2,1,0:T(8,128)(2,1)S(1)}, bf16[2,384,256]{2,1,0:T(8,128)(2,1)S(1)}) custom-call(s32[2,8]{1,0:T(2,128)} %chosen_ref.3, bf16[256,128]{1,0:T(8,128)(2,1)S(1)} %copy-done.3, bf16[256,128]{1,0:T(8,128)(2,1)S(1)} %copy-done.1, bf16[256,128]{1,0:T(8,128)(2,1)S(1)} %copy-done.2, ...), custom_call_target="tpu_custom_call" | custom-call | tf_op jit(solution)/shard_map/pallas_call | solution.py:184
  82.4 15.1 %all-to-all-start.2 = ((bf16[64,16,128]{2,1,0:T(8,128)(2,1)}), bf16[64,16,128]{2,1,0:T(8,128)(2,1)S(1)}, u32[]{:S(2)}, u32[]{:S(2)}) async-start(bf16[64,16,128]{2,1,0:T(8,128)(2,1)} %bitcast.9), calls=%async_computation.2 | async-start | bytes 524288 | tf_op jit(solution)/shard_map/all_to_all | solution.py:198
  97.4 1.0 shard_map.105
  98.4 1.3 collective-permute-start
  99.7 5.0 %collective-permute-done.partner_ref = bf16[256,128]{1,0:T(8,128)(2,1)S(1)} collective-permute-done((bf16[256,128]{1,0:T(8,128)(2,1)S(1)}, bf16[256,128]{1,0:T(8,128)(2,1)S(1)}, u32[]{:S(2)}, u32[]{:S(2)}) %collective-permute-start) | collective-permute-done | bytes 65568 | tf_op jit(solution)/shard_map/ppermute | solution.py:245
  104.7 0.0 collective-permute-done.5.other_ref
  104.7 15.2 %all-to-all-done.2 = bf16[64,16,128]{2,1,0:T(8,128)(2,1)S(1)} async-done(((bf16[64,16,128]{2,1,0:T(8,128)(2,1)}), bf16[64,16,128]{2,1,0:T(8,128)(2,1)S(1)}, u32[]{:S(2)}, u32[]{:S(2)}) %all-to-all-start.2) | async-done | bytes 262176 | tf_op jit(solution)/shard_map/all_to_all | solution.py:198
  119.9 2.8 %shard_map.108 = bf16[4,20,32,128]{3,2,1,0:T(8,128)(2,1)S(1)} custom-call(s32[1]{0:T(128)} %bitcast.6.y_ref, s32[1]{0:T(128)} %bitcast.7.x_ref, s32[1]{0:T(128)} %bitcast.8.c_ref, f32[8,128]{1,0:T(8,128)S(1)} %get-tuple-element.18.ids_ref, bf16[1024,128]{1,0:T(8,128)(2,1)S(1)} %bitcast.23, bf16[2,256,128]{2,1,0:T(8,128)(2,1)S(1)} %get-tuple-element.20.own_ref, ...), custom_call_target="tpu_custom_call" | custom-call | tf_op jit(solution)/shard_map/pallas_call | solution.py:184
  122.7 12.0 %all_to_all.26.got_ref = bf16[4,20,32,128]{3,2,1,0:T(8,128)(2,1)S(1)} all-to-all(bf16[4,20,32,128]{3,2,1,0:T(8,128)(2,1)S(1)} %shard_map.108), channel_id=1, replica_groups=mesh['z'=16,'y'=4,'x'=4,'c'=2] {'y'}, dimensions={0} | all-to-all | bytes 1310720 | tf_op jit(solution)/shard_map/all_to_all | solution.py:198
  134.7 0.1 shard_map.109
  134.8 22.7 %all_to_all.27.got_ref = bf16[16,64,128]{2,1,0:T(8,128)(2,1)S(1)} all-to-all(bf16[16,64,128]{2,1,0:T(8,128)(2,1)S(1)} %shard_map.109), channel_id=1, replica_groups=mesh['z'=16,'y'=4,'x'=4,'c'=2] {'z'}, dimensions={0} | all-to-all | bytes 524288 | tf_op jit(solution)/shard_map/all_to_all | solution.py:198
  157.5 0.9 shard_map.110
  (3 shorter events, 0.1 us)
Async XLA Ops:
  45.3 5.8 %copy-start = (bf16[256,256]{1,0:T(8,128)(2,1)S(1)}, bf16[256,256]{1,0:T(8,128)(2,1)}, u32[]{:S(2)}) copy-start(bf16[256,256]{1,0:T(8,128)(2,1)} %normed_ref.5) | copy-start | bytes 393220
  45.3 34.7 %all-to-all-start.1 = ((bf16[64,16,128]{2,1,0:T(8,128)(2,1)}), bf16[64,16,128]{2,1,0:T(8,128)(2,1)S(1)}, u32[]{:S(2)}, u32[]{:S(2)}) async-start(bf16[64,16,128]{2,1,0:T(8,128)(2,1)} %bitcast.4), calls=%async_computation.1 | async-start | bytes 524288 | tf_op jit(solution)/shard_map/all_to_all | solution.py:198
  51.2 7.2 %collective-permute-start.1 = (bf16[512,128]{1,0:T(8,128)(2,1)S(1)}, bf16[512,128]{1,0:T(8,128)(2,1)S(1)}, u32[]{:S(2)}, u32[]{:S(2)}) collective-permute-start(bf16[512,128]{1,0:T(8,128)(2,1)S(1)} %shard_map.106), channel_id=1, source_target_pairs={{0,8},{8,0},{16,24},{24,16},{1,9},{9,1},{17,25},{25,17},{2,10},{10... | collective-permute-start | bytes 393224 | tf_op jit(solution)/shard_map/ppermute | solution.py:207
  58.7 13.9 %collective-permute-start.4 = (bf16[2,128,512]{2,1,0:T(8,128)(2,1)S(1)}, bf16[2,128,512]{2,1,0:T(8,128)(2,1)S(1)}, u32[]{:S(2)}, u32[]{:S(2)}) collective-permute-start(bf16[2,128,512]{2,1,0:T(8,128)(2,1)S(1)} %shard_map.107), channel_id=1, source_target_pairs={{0,6},{2,0},{4,2},{6,4},{1,7},{3,1},{5,3},{7,5},{8,14},{10,8},{12,... | collective-permute-start | bytes 786440 | tf_op jit(solution)/shard_map/ppermute | solution.py:203
  63.4 11.7 %collective-permute-start.3 = (bf16[2,128,512]{2,1,0:T(8,128)(2,1)S(1)}, bf16[2,128,512]{2,1,0:T(8,128)(2,1)S(1)}, u32[]{:S(2)}, u32[]{:S(2)}) collective-permute-start(bf16[2,128,512]{2,1,0:T(8,128)(2,1)S(1)} %shard_map.107), channel_id=1, source_target_pairs={{0,4},{2,6},{4,0},{6,2},{1,5},{3,7},{5,1},{7,3},{8,12},{10,14},{12... | collective-permute-start | bytes 786440 | tf_op jit(solution)/shard_map/ppermute | solution.py:203
  66.1 11.8 %collective-permute-start.2 = (bf16[2,128,512]{2,1,0:T(8,128)(2,1)S(1)}, bf16[2,128,512]{2,1,0:T(8,128)(2,1)S(1)}, u32[]{:S(2)}, u32[]{:S(2)}) collective-permute-start(bf16[2,128,512]{2,1,0:T(8,128)(2,1)S(1)} %shard_map.107), channel_id=1, source_target_pairs={{0,2},{2,4},{4,6},{6,0},{1,3},{3,5},{5,7},{7,1},{8,10},{10,12},{12... | collective-permute-start | bytes 786440 | tf_op jit(solution)/shard_map/ppermute | solution.py:203
  77.9 2.1 %copy-start.1 = (bf16[256,128]{1,0:T(8,128)(2,1)S(1)}, bf16[256,128]{1,0:T(8,128)(2,1)}, u32[]{:S(2)}) copy-start(bf16[256,128]{1,0:T(8,128)(2,1)} %keys_ref.5) | copy-start | bytes 196612
  77.9 2.1 %copy-start.2 = (bf16[256,128]{1,0:T(8,128)(2,1)S(1)}, bf16[256,128]{1,0:T(8,128)(2,1)}, u32[]{:S(2)}) copy-start(bf16[256,128]{1,0:T(8,128)(2,1)} %values_ref.3) | copy-start | bytes 196612
  77.9 2.1 %copy-start.3 = (bf16[256,128]{1,0:T(8,128)(2,1)S(1)}, bf16[256,128]{1,0:T(8,128)(2,1)}, u32[]{:S(2)}) copy-start(bf16[256,128]{1,0:T(8,128)(2,1)} %queries_ref.3) | copy-start | bytes 196612
  77.9 2.1 %copy-start.4 = (bf16[256,128]{1,0:T(8,128)(2,1)S(1)}, bf16[256,128]{1,0:T(8,128)(2,1)}, u32[]{:S(2)}) copy-start(bf16[256,128]{1,0:T(8,128)(2,1)} %grad_ref.3) | copy-start | bytes 196612
  77.9 2.1 %copy-start.5 = (f32[2,256]{1,0:T(2,128)S(1)}, f32[2,256]{1,0:T(2,128)}, u32[]{:S(2)}) copy-start(f32[2,256]{1,0:T(2,128)} %sums_ref.1) | copy-start | bytes 6148
  78.1 26.7 %collective-permute-start.5 = (bf16[4,2,128,512]{3,2,1,0:T(8,128)(2,1)S(1)}, bf16[4,2,128,512]{3,2,1,0:T(8,128)(2,1)}, u32[]{:S(2)}, u32[]{:S(2)}) collective-permute-start(bf16[4,2,128,512]{3,2,1,0:T(8,128)(2,1)S(1)} %pad_maximum_fusion.mine_ref), channel_id=1, source_target_pairs={{0,1},{1,0},{2,3},{3,2},{4,5},{5,4},{6,7},{7,6},{8,9},{9,8},{10,11... | collective-permute-start | bytes 3145736 | tf_op jit(solution)/shard_map/ppermute | solution.py:203
  82.4 37.5 %all-to-all-start.2 = ((bf16[64,16,128]{2,1,0:T(8,128)(2,1)}), bf16[64,16,128]{2,1,0:T(8,128)(2,1)S(1)}, u32[]{:S(2)}, u32[]{:S(2)}) async-start(bf16[64,16,128]{2,1,0:T(8,128)(2,1)} %bitcast.9), calls=%async_computation.2 | async-start | bytes 524288 | tf_op jit(solution)/shard_map/all_to_all | solution.py:198
  98.4 6.3 %collective-permute-start = (bf16[256,128]{1,0:T(8,128)(2,1)S(1)}, bf16[256,128]{1,0:T(8,128)(2,1)S(1)}, u32[]{:S(2)}, u32[]{:S(2)}) collective-permute-start(bf16[256,128]{1,0:T(8,128)(2,1)S(1)} %slice_bitcast_fusion), channel_id=1, source_target_pairs={{8,0},{24,16},{9,1},{25,17},{10,2},{26,18},{11,3},{27,19},{12,4},{... | collective-permute-start | bytes 196616 | tf_op jit(solution)/shard_map/ppermute | solution.py:245
